TPU v7x, 32 devices: a whole 2x2x4 slice. The times are simulated.
32 devices in a mesh: sp: 8 (over z, y), tp: 4 (over x, core).
Axes of the slice: x: 2, y: 2, z: 4, core: 2. Of those that a mesh axis runs over, the one named last changes fastest.
Arguments:
- stream_in: bfloat16 [2048, 4096], P(('sp', 'tp')), may hold values from -6 to 6
- q_first: bfloat16 [2048, 1024], P('sp', 'tp'), may hold values from -110 to 110
- q_second: bfloat16 [2048, 1024], P('sp', 'tp'), may hold values from -110 to 110
- k_first: bfloat16 [2048, 512], P('sp', 'tp'), may hold values from -7 to 7
- k_second: bfloat16 [2048, 512], P('sp', 'tp'), may hold values from -7 to 7
- values: bfloat16 [2048, 1024], P('sp', 'tp'), may hold values from -6 to 6
- head_lambda: float32 [8], P('tp'), may hold values from 0.3 to 0.8
- w_out: bfloat16 [2048, 4096], P('tp'), may hold values from -0.125 to 0.125
- norm_gain: float32 [4096], replicated, may hold values from 0.1 to 1.9
- routes: int32 [2048, 4], P(('sp', 'tp')), may hold values from 0 to 7, all different within a row; in each aligned block of 64 rows (0 to 63, 64 to 127, ...) at most 48 rows name the same one
- route_w: float32 [2048, 4], P(('sp', 'tp')), may hold values from 0.2 to 1
- w_gate: bfloat16 [8, 4096, 128], P('sp'), may hold values from -0.09375 to 0.09375
- w_up: bfloat16 [8, 4096, 128], P('sp'), may hold values from -0.09375 to 0.09375
- w_down: bfloat16 [8, 128, 4096], P('sp'), may hold values from -0.5 to 0.5
- s_gate: bfloat16 [4096, 512], P(None, 'tp'), may hold values from -0.09375 to 0.09375
- s_up: bfloat16 [4096, 512], P(None, 'tp'), may hold values from -0.09375 to 0.09375
- s_down: bfloat16 [512, 4096], P('tp'), may hold values from -0.25 to 0.25
Outputs:
- layer_out: bfloat16 [2048, 4096], P(('sp', 'tp'))
Inputs may be any that keep to these rules, and one draw needn't show every extreme that they name: `routes`: each row names 4 different experts. Within the rows of one device (aligned blocks of 64 rows) no expert is named more than 48 times, and in some blocks one expert is named exactly 48 times.
All inputs are finite; a program needn't handle non-finite values.
Results may differ from a plain program's by a relative error of at most 0.017.
Values may be sent and summed in bfloat16 or wider, within the bound.
A program may use at most 128 MiB of HBM per device.

v0:
```python
import functools
import math

import jax
import jax.numpy as jnp
from jax import lax
from jax.experimental import pallas as pl
from jax.experimental.pallas import tpu as pltpu
from jax.sharding import PartitionSpec as P

HEAD = 128


FLOOR = -1e30


def absorb(state, first_q, second_q, first_k, second_k, value_rows, query_pos, key_pos):
    allowed = key_pos[None, :] <= query_pos[:, None]
    scale = first_q.shape[-1] ** (-0.5)
    result = []
    pairs = ((first_q, first_k), (second_q, second_k))
    for index in range(2):
        query_rows, key_rows = pairs[index]
        peak, total, accum = (state[3 * index], state[3 * index + 1], state[3 * index + 2])
        scores = (
            jnp.einsum("qagd,kad->agqk", query_rows, key_rows, preferred_element_type=jnp.float32)
            * scale
        )
        scores = jnp.where(allowed, scores, FLOOR)
        raised = jnp.maximum(peak, scores.max(-1))
        weights = jnp.where(allowed, jnp.exp(scores - raised[..., None]), 0.0)
        fade = jnp.exp(peak - raised)
        total = total * fade + weights.sum(-1)
        accum = accum * fade[..., None] + jnp.einsum(
            "agqk,kad->agqd",
            weights.astype(jnp.bfloat16),
            value_rows,
            preferred_element_type=jnp.float32,
        )
        result += [raised, total, accum]
    return tuple(result)


def empty_state(kv_local, group, count, value_dim):
    peaks = jnp.full((kv_local, group, count), FLOOR, jnp.float32)
    sums = jnp.zeros((kv_local, group, count), jnp.float32)
    accums = jnp.zeros((kv_local, group, count, value_dim), jnp.float32)
    return (peaks, sums, accums, peaks, sums, accums)


def fold_rows(state, first_q, second_q, query_pos, last_row, pieces, start):
    first_k, second_k, value_rows = pieces
    length = first_k.shape[0]
    kv_local = first_q.shape[1]
    value_dim = value_rows.shape[1] // kv_local
    span = math.gcd(length, 2048)

    def sweep(current):

        def visit(block, inner):
            begin = block * span
            key_one = lax.dynamic_slice_in_dim(first_k, begin, span, 0).reshape(
                span, kv_local, HEAD
            )
            key_two = lax.dynamic_slice_in_dim(second_k, begin, span, 0).reshape(
                span, kv_local, HEAD
            )
            value_part = lax.dynamic_slice_in_dim(value_rows, begin, span, 0).reshape(
                span, kv_local, value_dim
            )
            key_pos = begin + jnp.arange(span, dtype=jnp.int32)
            return absorb(
                inner, first_q, second_q, key_one, key_two, value_part, query_pos, key_pos
            )

        return lax.fori_loop(0, length // span, visit, current)

    def unchanged(current):
        return current

    return lax.cond(start <= last_row, sweep, unchanged, state)


def finish_heads(final, head_lambda):
    kv_local, group, count, value_dim = final[2].shape
    weight = head_lambda.reshape(kv_local, group, 1, 1)
    head_out = final[2] / final[1][..., None] - weight * final[5] / final[4][..., None]
    head_out = head_out * lax.rsqrt(jnp.mean(head_out * head_out, axis=-1, keepdims=True) + 1e-05)
    return (
        head_out.transpose(2, 0, 1, 3)
        .reshape(count, kv_local * group * value_dim)
        .astype(jnp.bfloat16)
    )


def shared_part(normed, s_gate, s_up, s_down):
    piece = lax.all_gather(normed, "tp", axis=0, tiled=True)
    gate_part = jnp.dot(piece, s_gate, preferred_element_type=jnp.float32)
    up_part = jnp.dot(piece, s_up, preferred_element_type=jnp.float32)
    hidden = (jax.nn.silu(gate_part) * up_part).astype(jnp.bfloat16)
    terms = jnp.dot(hidden, s_down, preferred_element_type=jnp.float32)
    return lax.psum_scatter(
        terms.astype(jnp.bfloat16), "tp", scatter_dimension=0, tiled=True
    ).astype(jnp.float32)


def routed_part(normed, routes, route_w, w_gate, w_up, w_down):
    rows, topk = routes.shape
    local_experts = w_gate.shape[0]
    experts = local_experts * lax.axis_size("sp")
    slots = max(2, 3 * rows * topk // (2 * experts))
    flat_ids = routes.reshape(-1)
    hits = (flat_ids[:, None] == jnp.arange(experts, dtype=jnp.int32)[None, :]).astype(jnp.int32)
    slot_of = jnp.sum(jnp.cumsum(hits, axis=0) * hits, axis=1) - 1
    target = flat_ids * slots + slot_of
    placing = jnp.any(
        jnp.arange(experts * slots, dtype=jnp.int32)[:, None, None]
        == target.reshape(rows, topk)[None, :, :],
        axis=-1,
    ).astype(jnp.bfloat16)
    outgoing = (
        jnp.dot(placing, normed, preferred_element_type=jnp.float32)
        .astype(jnp.bfloat16)
        .reshape(experts, slots, normed.shape[1])
    )
    arrived = lax.all_to_all(outgoing, "sp", split_axis=0, concat_axis=0, tiled=True)
    sources = arrived.shape[0] // local_experts
    grouped = arrived.reshape(sources, local_experts, arrived.shape[1], arrived.shape[2])
    gate_part = jnp.einsum("sjcd,jdf->sjcf", grouped, w_gate, preferred_element_type=jnp.float32)
    up_part = jnp.einsum("sjcd,jdf->sjcf", grouped, w_up, preferred_element_type=jnp.float32)
    hidden = (jax.nn.silu(gate_part) * up_part).astype(jnp.bfloat16)
    result = jnp.einsum(
        "sjcf,jfd->sjcd", hidden, w_down, preferred_element_type=jnp.float32
    ).astype(jnp.bfloat16)
    returned = lax.all_to_all(
        result.reshape(arrived.shape), "sp", split_axis=0, concat_axis=0, tiled=True
    )
    picked = (
        returned.reshape(experts * slots, normed.shape[1])[target]
        .reshape(rows, topk, normed.shape[1])
        .astype(jnp.float32)
    )
    return jnp.sum(picked * route_w[..., None], axis=1)


def local(
    stream_in,
    q_first,
    q_second,
    k_first,
    k_second,
    values,
    head_lambda,
    w_out,
    norm_gain,
    routes,
    route_w,
    w_gate,
    w_up,
    w_down,
    s_gate,
    s_up,
    s_down,
):
    seq_rows = q_first.shape[0]
    kv_local = k_first.shape[1] // HEAD
    heads_local = q_first.shape[1] // HEAD
    group = heads_local // kv_local
    value_dim = values.shape[1] // kv_local
    offset = lax.axis_index("sp") * seq_rows
    query_pos = offset + jnp.arange(seq_rows, dtype=jnp.int32)
    last_row = offset + seq_rows - 1
    first_q = q_first.reshape(seq_rows, kv_local, group, HEAD)
    second_q = q_second.reshape(seq_rows, kv_local, group, HEAD)
    start_state = empty_state(kv_local, group, seq_rows, value_dim)
    folded_state = fold_rows(
        start_state,
        first_q,
        second_q,
        query_pos,
        last_row,
        (
            lax.all_gather(k_first, "sp", axis=0, tiled=True),
            lax.all_gather(k_second, "sp", axis=0, tiled=True),
            lax.all_gather(values, "sp", axis=0, tiled=True),
        ),
        jnp.int32(0),
    )
    attn_rows = finish_heads(folded_state, head_lambda)
    attn = lax.psum_scatter(
        jnp.dot(attn_rows, w_out, preferred_element_type=jnp.float32).astype(jnp.bfloat16),
        "tp",
        scatter_dimension=0,
        tiled=True,
    ).astype(jnp.float32)
    resid = (stream_in.astype(jnp.float32) + attn).astype(jnp.bfloat16)
    stream = lax.optimization_barrier(resid).astype(jnp.float32)
    normed = (
        stream * lax.rsqrt(jnp.mean(stream * stream, axis=-1, keepdims=True) + 1e-06) * norm_gain
    ).astype(jnp.bfloat16)
    routed = routed_part(normed, routes, route_w, w_gate, w_up, w_down)
    shared = shared_part(normed, s_gate, s_up, s_down)
    return (stream + routed + shared).astype(jnp.bfloat16)


def mesh_copy(src, dst, send_sem, recv_sem, axis, target):
    return pltpu.make_async_remote_copy(
        src_ref=src,
        dst_ref=dst,
        send_sem=send_sem,
        recv_sem=recv_sem,
        device_id={axis: target},
        device_id_type=pl.DeviceIdType.MESH,
    )


def greet(axis, target):
    pl.semaphore_signal(
        pltpu.get_barrier_semaphore(),
        inc=1,
        device_id={axis: target},
        device_id_type=pl.DeviceIdType.MESH,
    )


def near_kernel(
    n, nt, group, pieces,
    q_one, q_two, k_one, k_two, val, lam, w_out_h, stream, gain, mix,
    gate_h, up_h, s_gate_h, s_up_h, down_h, s_down_h,
    out,
    stacked, keys_one, keys_two, vals, peak, total, accum, rows_in,
    w, order, out_one, in_one, out_two, in_two, resid,
    gates, ups, s_gate, s_up, wall, gathered, beside, out_hid, in_hid, out_sh, in_sh, units,
    load, send_kv, recv_kv, send_one, recv_one, send_two, recv_two,
    send_g, recv_g, send_d, recv_d, send_sd, recv_sd,
    send_x, recv_x, send_b, recv_b, send_h, recv_h, send_s, recv_s,
):
    me, mine = lax.axis_index("sp"), lax.axis_index("tp")
    place, side = me // 2, me % 2
    far, core = mine // 2, mine % 2
    depth, half = n // 2, nt // 2
    pair, partner = me + 1 - 2 * side, mine + 1 - 2 * core
    above, below = place < depth - 1, place > 0
    seq = q_one.shape[0]
    rows, width = stream.shape
    hid, wide = down_h.shape[0], s_down_h.shape[0]
    scale = HEAD ** (-0.5)

    def fars(o):
        return 2 * ((far + o) % half) + core

    def column(o):
        return 2 * ((place + o) % depth) + side

    loads = [
        pltpu.make_async_copy(source, target, load.at[i])
        for i, (source, target) in enumerate(
            (
                (w_out_h, w),
                (gate_h, gates.at[0]),
                (up_h, ups.at[0]),
                (s_gate_h, s_gate),
                (s_up_h, s_up),
                (down_h, wall.at[pl.ds(pl.multiple_of(me * hid, hid), hid)]),
                (s_down_h, wall.at[pl.ds(pl.multiple_of(n * hid + mine * wide, wide), wide)]),
            )
        )
    ]
    for o in range(1, depth):
        greet("sp", column(o))
    greet("sp", pair)
    for o in range(1, half):
        greet("tp", fars(o))
    greet("tp", partner)
    pl.semaphore_wait(pltpu.get_barrier_semaphore(), depth + half)

    sources = (k_one, k_two, val)
    held = (keys_one, keys_two, vals)

    def copies(block, way, target, own):
        return [
            mesh_copy(
                sources[a] if own else held[a].at[block],
                held[a].at[block],
                send_kv.at[way, a, block],
                recv_kv.at[a, block],
                "sp",
                target,
            )
            for a in range(3)
        ]

    def start(block, way, target, own=False):
        for one in copies(block, way, target, own):
            one.start()

    def arrive(block):
        for one in copies(block, 0, pair, False):
            one.wait_recv()

    share = width // 2
    share_at = pl.ds(pl.multiple_of(core * share, share), share)
    other_at = pl.ds(pl.multiple_of((1 - core) * share, share), share)

    def pair_weights():
        return [
            mesh_copy(
                h.at[share_at], v.at[1, share_at], send_g.at[0, i], recv_g.at[0, i], "sp", pair
            )
            for i, (h, v) in enumerate(((gate_h, gates), (up_h, ups)))
        ]

    def pair_weights_on(at):
        return [
            mesh_copy(
                v.at[1, at], v.at[1, at], send_g.at[1, i], recv_g.at[1, i], "tp", partner
            )
            for i, v in enumerate((gates, ups))
        ]

    part = hid // 2

    def down_at(block, c):
        return wall.at[pl.ds(pl.multiple_of(block * hid + c * part, part), part)]

    def down_own(way, target, axis="sp"):
        return mesh_copy(
            down_h.at[pl.ds(pl.multiple_of(core * part, part), part)],
            down_at(me, core),
            send_d.at[way],
            recv_d.at[0, me],
            axis,
            target,
        )

    def down_pair(block):
        return mesh_copy(
            down_at(block, core),
            down_at(block, core),
            send_d.at[depth + block],
            recv_d.at[0, block],
            "sp",
            pair,
        )

    def down_core(block, c):
        return mesh_copy(
            down_at(block, c),
            down_at(block, c),
            send_d.at[depth + n + block],
            recv_d.at[1, block],
            "tp",
            partner,
        )

    def sd_at(u):
        return wall.at[pl.ds(pl.multiple_of(n * hid + u * wide, wide), wide)]

    def sd_own(way, target):
        return mesh_copy(s_down_h, sd_at(mine), send_sd.at[way], recv_sd.at[mine], "tp", target)

    def sd_on(o, u):
        return mesh_copy(
            sd_at(u), sd_at(u), send_sd.at[half + o - 1], recv_sd.at[u], "tp", partner
        )

    @pl.when(above)
    def _():
        start(me, 0, me + 2, True)

    @pl.when(side == 0)
    def _():
        start(me, 1, pair, True)

    for one in loads:
        one.start()
    for o in range(1, half):
        sd_own(o, fars(o)).start()
    sd_own(0, partner).start()
    for o in range(1, depth):

        @pl.when(place + o >= depth)
        def _():
            down_own(o, column(o)).start()

    for index, q in enumerate((q_one, q_two)):
        for h in range(group):
            stacked[index, h * seq : (h + 1) * seq, :] = q[:, h * HEAD : (h + 1) * HEAD]

    def scores_of(index, keys):
        return (
            lax.dot_general(
                stacked[index], keys, (((1,), (1,)), ((), ())), preferred_element_type=jnp.float32
            )
            * scale
        )

    spread = (group * seq, seq)
    row_of = lax.broadcasted_iota(jnp.int32, spread, 0) % seq
    allowed = lax.broadcasted_iota(jnp.int32, spread, 1) <= row_of
    for index, keys in enumerate((k_one, k_two)):
        scores = jnp.where(allowed, scores_of(index, keys[...]), FLOOR)
        top = jnp.max(scores, axis=-1, keepdims=True)
        weights = jnp.exp(scores - top)
        peak[index] = top
        total[index] = jnp.sum(weights, axis=-1, keepdims=True)
        accum[index] = jnp.dot(
            weights.astype(jnp.bfloat16), val[...], preferred_element_type=jnp.float32
        )

    def fold(block):
        for index in range(2):
            scores = scores_of(index, held[index][block])
            old = peak[index]
            top = jnp.maximum(old, jnp.max(scores, axis=-1, keepdims=True))
            weights = jnp.exp(scores - top)
            fade = jnp.exp(old - top)
            peak[index] = top
            total[index] = total[index] * fade + jnp.sum(weights, axis=-1, keepdims=True)
            accum[index] = accum[index] * fade + jnp.dot(
                weights.astype(jnp.bfloat16), vals[block], preferred_element_type=jnp.float32
            )

    def visit(e, carry):
        @pl.when(place >= e)
        def _():
            block = me - 2 * e
            arrive(block)

            @pl.when(above)
            def _():
                start(block, 0, me + 2)

            start(block, 1, pair)
            fold(block)

        @pl.when((place >= e - 1) & ((e > 1) | (side == 1)))
        def _():
            block = pair - 2 * (e - 1)
            arrive(block)
            fold(block)

        @pl.when(e == jnp.maximum(place, 1))
        def _():
            for one in pair_weights():
                one.start()
            down_own(0, pair).start()

        return carry

    lax.fori_loop(1, depth + 1, visit, 0)

    @pl.when(above)
    def _():
        down_own(1, me + 2).start()

    def down_up(block):
        return mesh_copy(
            down_at(block, core),
            down_at(block, core),
            send_d.at[depth + 2 * n + block],
            recv_d.at[0, block],
            "sp",
            me + 2,
        )

    def lift(d):
        @pl.when((place >= d) & above)
        def _():
            down_up(me - 2 * d).wait_recv()
            down_up(me - 2 * d).start()

    for h in range(group):
        cut = slice(h * seq, (h + 1) * seq)
        head = accum[0, cut, :] / total[0, cut, :] - lam[h] * (
            accum[1, cut, :] / total[1, cut, :]
        )
        head = head * lax.rsqrt(jnp.mean(head * head, axis=-1, keepdims=True) + 1e-05)
        size = head.shape[1]
        rows_in[:, h * size : (h + 1) * size] = head.astype(jnp.bfloat16)

    for o in range(half):
        base = 2 * ((far + o) % half)
        for which, parity in enumerate((1 - core, core)):
            begin = pl.multiple_of((base + parity) * rows, rows)
            order[which, o * rows : (o + 1) * rows, :] = rows_in[pl.ds(begin, rows), :]

    first = [
        mesh_copy(out_one.at[i], in_one.at[i], send_one.at[i], recv_one.at[i], "tp", partner)
        for i in range(pieces)
    ]
    second = [
        [
            mesh_copy(
                out_two.at[o, i],
                in_two.at[o, i],
                send_two.at[o, i],
                recv_two.at[o, i],
                "tp",
                fars(o + 1),
            )
            for o in range(half - 1)
        ]
        for i in range(pieces)
    ]
    span = width // pieces
    loads[0].wait()
    for i in range(pieces):
        out_one[i] = jnp.dot(
            order[0], w[:, i * span : (i + 1) * span], preferred_element_type=jnp.float32
        ).astype(jnp.bfloat16)
        first[i].start()
    lift(1)
    kept = []
    for i in range(pieces):
        sums = jnp.dot(
            order[1], w[:, i * span : (i + 1) * span], preferred_element_type=jnp.float32
        )
        first[i].wait_recv()
        sums = sums + in_one[i].astype(jnp.float32)
        for o in range(half - 1):
            out_two[o, i] = sums[(o + 1) * rows : (o + 2) * rows].astype(jnp.bfloat16)
            second[i][o].start()
        kept.append(sums[:rows])
    for d in range(2, depth):
        lift(d)
    for o in range(1, half):
        u = fars(o)
        sd_on(o, u).wait_recv()
        sd_on(o, u).start()
    squares = jnp.zeros((rows, 1), jnp.float32)
    for i in range(pieces):
        cut = slice(i * span, (i + 1) * span)
        sums = kept[i]
        for o in range(half - 1):
            second[i][o].wait_recv()
            sums = sums + in_two[o, i].astype(jnp.float32)
        sums = (stream[:, cut].astype(jnp.float32) + sums).astype(jnp.bfloat16)
        resid[:, cut] = sums
        sums = sums.astype(jnp.float32)
        squares = squares + jnp.sum(sums * sums, axis=-1, keepdims=True)
    shrink = lax.rsqrt(squares / width + 1e-06)
    for i in range(pieces):
        cut = slice(i * span, (i + 1) * span)
        gathered[place, :, cut] = (
            resid[:, cut].astype(jnp.float32) * shrink * gain[:, cut]
        ).astype(jnp.bfloat16)

    chunk = rows // 2

    def row_copy(spot, way, target, c):
        some = gathered.at[spot, pl.ds(c * chunk, chunk)]
        return mesh_copy(
            some,
            some,
            send_x.at[way, c, spot],
            recv_x.at[c, spot],
            "sp",
            target,
        )

    def beside_own(way, target):
        return mesh_copy(
            gathered.at[place], beside.at[mine], send_b.at[way], recv_b.at[mine], "tp", target
        )

    def beside_on(o, u):
        return mesh_copy(
            beside.at[u], beside.at[u], send_b.at[half + o - 1], recv_b.at[u], "tp", partner
        )

    for c in range(2):
        pl.when(above)(lambda: row_copy(place, 0, me + 2, c).start())
        pl.when(below)(lambda: row_copy(place, 1, me - 2, c).start())

    for o in range(1, half):
        beside_own(o, fars(o)).start()
    beside_own(0, partner).start()

    def pass_down(e):
        def one(block, fresh):
            pl.when(fresh)(lambda: down_pair(block).wait_recv())
            down_pair(block).start()
            down_core(block, core).start()

        pl.when(place >= e)(lambda: one(me - 2 * e, jnp.logical_not(above)))
        pl.when(place + e < depth)(lambda: one(me + 2 * e, place >= 0))

    def collect(e):
        def one(block):
            down_pair(block).wait_recv()
            down_core(block, core).start()

        pl.when(place >= e)(lambda: one(pair - 2 * e))
        pl.when(place + e < depth)(lambda: one(pair + 2 * e))

    for one, onward in zip(pair_weights(), pair_weights_on(share_at)):
        one.wait_recv()
        onward.start()
    pass_down(1)
    def hidden_of(block_rows, g, u):
        gate_part = jnp.dot(block_rows, g, preferred_element_type=jnp.float32)
        up_part = jnp.dot(block_rows, u, preferred_element_type=jnp.float32)
        return (gate_part / (1.0 + jnp.exp(-gate_part)) * up_part).astype(jnp.bfloat16)

    for i in range(1, 5):
        loads[i].wait()
    in_sh[mine] = hidden_of(gathered[place], s_gate[...], s_up[...])
    in_hid[place, side] = hidden_of(gathered[place], gates[0], ups[0])

    def hid_copy(spot):
        return mesh_copy(
            out_hid.at[spot], in_hid.at[place], send_h.at[spot], recv_h.at[place], "sp",
            2 * spot + side,
        )

    def serve(spot):
        out_hid[spot, side] = hidden_of(gathered[spot], gates[0], ups[0])
        out_hid[spot, 1 - side] = hidden_of(gathered[spot], gates[1], ups[1])
        hid_copy(spot).start()

    def sh_copy(u):
        return mesh_copy(
            out_sh.at[u], in_sh.at[mine], send_s.at[u], recv_s.at[mine], "tp", u
        )

    def answer(u):
        out_sh[u] = hidden_of(beside[u], s_gate[...], s_up[...])
        sh_copy(u).start()

    def turn(e, carry):
        low, high = place >= e, place + e < depth

        for c in range(2):

            @pl.when(low)
            def _():
                row_copy(place - e, 0, pair, c).wait_recv()
                pl.when(above)(lambda: row_copy(place - e, 0, me + 2, c).start())

            @pl.when(high)
            def _():
                row_copy(place + e, 0, pair, c).wait_recv()
                pl.when(below)(lambda: row_copy(place + e, 1, me - 2, c).start())

        pass_down(e + 1)

        @pl.when(e == 1)
        def _():
            down_pair(pair).wait_recv()
            down_core(pair, core).start()
            for one in pair_weights_on(other_at):
                one.wait_recv()

        @pl.when(low)
        def _():
            serve(place - e)

        @pl.when(high)
        def _():
            serve(place + e)

        @pl.when(e > 1)
        def _():
            collect(e - 1)

        @pl.when(e == 1)
        def _():
            in_hid[place, 1 - side] = hidden_of(gathered[place], gates[1], ups[1])
            for o in range(1, half):
                u = fars(o)
                beside_on(o, u).wait_recv()
                beside_on(o, u).start()
                answer(u)
            for o in range(half):
                u = 2 * ((far + o) % half) + 1 - core
                beside_on(1, u).wait_recv()
                answer(u)

        return carry

    lax.fori_loop(1, depth, turn, 0)

    collect(depth - 1)

    for o in range(1, depth):
        spot = (place + o) % depth
        mesh_copy(
            out_hid.at[spot], in_hid.at[spot], send_h.at[spot], recv_h.at[spot], "sp",
            2 * spot + side,
        ).wait_recv()
    for o in range(1, nt):
        u = (mine + o) % nt
        mesh_copy(
            out_sh.at[u], in_sh.at[u], send_s.at[u], recv_s.at[u], "tp", u
        ).wait_recv()
    for j in range(n):
        units[:, j * hid : (j + 1) * hid] = (
            in_hid[j // 2, j % 2].astype(jnp.float32) * mix[:, j : j + 1]
        ).astype(jnp.bfloat16)
    for j in range(nt):
        units[:, n * hid + j * wide : n * hid + (j + 1) * wide] = in_sh[j]

    loads[5].wait()
    loads[6].wait()
    for o in range(half):
        sd_on(1, 2 * ((far + o) % half) + 1 - core).wait_recv()

    def receive_down(block, carry):
        @pl.when(block != me)
        def _():
            down_core(block, 1 - core).wait_recv()

        return carry

    lax.fori_loop(0, n, receive_down, 0)
    for i in range(2 * pieces):
        cut = slice(i * span // 2, (i + 1) * span // 2)
        out[:, cut] = (
            resid[:, cut].astype(jnp.float32)
            + jnp.dot(units[...], wall[:, cut], preferred_element_type=jnp.float32)
        ).astype(jnp.bfloat16)

    def settle(e, carry):
        @pl.when(place >= e)
        def _():
            block = me - 2 * e

            @pl.when(above)
            def _():
                for one in copies(block, 0, me + 2, False):
                    one.wait_send()
                for c in range(2):
                    row_copy(place - e, 0, me + 2, c).wait_send()

                @pl.when(e > 0)
                def _():
                    down_up(block).wait_send()

            @pl.when((e > 0) | (side == 0))
            def _():
                for one in copies(block, 1, pair, False):
                    one.wait_send()

        @pl.when((place + e < depth) & below)
        def _():
            for c in range(2):
                row_copy(place + e, 1, me - 2, c).wait_send()

        @pl.when(e != place)
        def _():
            hid_copy(e).wait_send()
            down_pair(2 * e + side).wait_send()

        return carry

    lax.fori_loop(0, depth, settle, 0)

    def settle_down(block, carry):
        @pl.when(block != me)
        def _():
            down_core(block, core).wait_send()

        return carry

    lax.fori_loop(0, n, settle_down, 0)
    for i in range(pieces):
        first[i].wait_send()
        for o in range(half - 1):
            second[i][o].wait_send()
    for one in pair_weights() + pair_weights_on(share_at):
        one.wait_send()
    for o in range(1, depth):
        pl.when((place + o >= depth) | (o == 1))(lambda: down_own(o, column(o)).wait_send())
    down_own(0, pair).wait_send()
    sd_own(0, partner).wait_send()
    beside_own(0, partner).wait_send()
    for o in range(1, half):
        u = fars(o)
        sd_own(o, u).wait_send()
        sd_on(o, u).wait_send()
        beside_own(o, u).wait_send()
        beside_on(o, u).wait_send()
    for o in range(1, nt):
        sh_copy((mine + o) % nt).wait_send()


def near(
    stream_in,
    q_first,
    q_second,
    k_first,
    k_second,
    values,
    head_lambda,
    w_out,
    norm_gain,
    routes,
    route_w,
    w_gate,
    w_up,
    w_down,
    s_gate,
    s_up,
    s_down,
):
    n, nt = lax.axis_size("sp"), lax.axis_size("tp")
    depth, half = n // 2, nt // 2
    seq, rows, width = q_first.shape[0], stream_in.shape[0], stream_in.shape[1]
    group, value_dim = q_first.shape[1] // HEAD, values.shape[1]
    hid, wide = w_down.shape[1], s_down.shape[0]
    tall, features = group * seq, group * value_dim
    pieces = 4
    span = width // pieces
    chosen = routes[:, :, None] == jnp.arange(n, dtype=jnp.int32)[None, None, :]
    mix = jnp.sum(jnp.where(chosen, route_w[:, :, None], 0.0), axis=1)
    vmem = pl.BlockSpec(memory_space=pltpu.VMEM)
    smem = pl.BlockSpec(memory_space=pltpu.SMEM)
    hbm = pl.BlockSpec(memory_space=pl.ANY)
    low, high = jnp.bfloat16, jnp.float32
    dma = pltpu.SemaphoreType.DMA
    return pl.pallas_call(
        functools.partial(near_kernel, n, nt, group, pieces),
        out_shape=jax.ShapeDtypeStruct((rows, width), low),
        in_specs=[vmem] * 5 + [smem, hbm] + [vmem] * 3 + [hbm] * 6,
        out_specs=vmem,
        scratch_shapes=[
            pltpu.VMEM((2, tall, HEAD), low),
            pltpu.VMEM((n, seq, HEAD), low),
            pltpu.VMEM((n, seq, HEAD), low),
            pltpu.VMEM((n, seq, value_dim), low),
            pltpu.VMEM((2, tall, 1), high),
            pltpu.VMEM((2, tall, 1), high),
            pltpu.VMEM((2, tall, value_dim), high),
            pltpu.VMEM((seq, features), low),
            pltpu.VMEM((features, width), low),
            pltpu.VMEM((2, half * rows, features), low),
            pltpu.VMEM((pieces, half * rows, span), low),
            pltpu.VMEM((pieces, half * rows, span), low),
            pltpu.VMEM((half - 1, pieces, rows, span), low),
            pltpu.VMEM((half - 1, pieces, rows, span), low),
            pltpu.VMEM((rows, width), low),
            pltpu.VMEM((2, width, hid), low),
            pltpu.VMEM((2, width, hid), low),
            pltpu.VMEM((width, wide), low),
            pltpu.VMEM((width, wide), low),
            pltpu.VMEM((n * hid + nt * wide, width), low),
            pltpu.VMEM((depth, rows, width), low),
            pltpu.VMEM((nt, rows, width), low),
            pltpu.VMEM((depth, 2, rows, hid), low),
            pltpu.VMEM((depth, 2, rows, hid), low),
            pltpu.VMEM((nt, rows, wide), low),
            pltpu.VMEM((nt, rows, wide), low),
            pltpu.VMEM((rows, n * hid + nt * wide), low),
            dma((7,)),
            dma((2, 3, n)),
            dma((3, n)),
            dma((pieces,)),
            dma((pieces,)),
            dma((half - 1, pieces)),
            dma((half - 1, pieces)),
            dma((2, 2)),
            dma((2, 2)),
            dma((depth + 3 * n,)),
            dma((2, n)),
            dma((nt,)),
            dma((nt,)),
            dma((2, 2, depth)),
            dma((2, depth)),
            dma((nt,)),
            dma((nt,)),
            dma((depth,)),
            dma((depth,)),
            dma((nt,)),
            dma((nt,)),
        ],
        compiler_params=pltpu.CompilerParams(
            collective_id=0, has_side_effects=True, vmem_limit_bytes=60 << 20
        ),
        name="layer",
    )(
        q_first, q_second, k_first, k_second, values, head_lambda, w_out, stream_in,
        norm_gain.reshape(1, width), mix, w_gate[0], w_up[0], s_gate, s_up, w_down[0], s_down,
    )


def layer(*arrays):
    n, nt = lax.axis_size("sp"), lax.axis_size("tp")
    k_first, values, w_gate, w_down, s_down = (arrays[i] for i in (3, 5, 11, 13, 16))
    fits = (
        2 <= n <= 16
        and n % 2 == 0
        and nt >= 4
        and nt % 2 == 0
        and k_first.shape[1] == HEAD
        and w_gate.shape[0] == 1
        and w_down.shape[1] % (16 * nt) == 0
        and s_down.shape[0] % (16 * n) == 0
    )
    return near(*arrays) if fits else local(*arrays)


def solution(mesh):
    return jax.shard_map(
        layer,
        mesh=mesh,
        in_specs=(
            P(("sp", "tp"), None),
            P("sp", "tp"),
            P("sp", "tp"),
            P("sp", "tp"),
            P("sp", "tp"),
            P("sp", "tp"),
            P("tp"),
            P("tp", None),
            P(),
            P(("sp", "tp"), None),
            P(("sp", "tp"), None),
            P("sp", None, None),
            P("sp", None, None),
            P("sp", None, None),
            P(None, "tp"),
            P(None, "tp"),
            P("tp", None),
        ),
        out_specs=P(("sp", "tp"), None),
        check_vma=False,
    )
```

profile of v0, /device:TPU:0, one launch (start us, length us, event | category | flops | bytes accessed | tf_op | source)
XLA Modules:
  0.0 111.1 jit_solution(7398015712126830968)
XLA Ops:
  0.0 0.7 select_reduce_fusion
  0.7 0.7 copy.20.mix
  1.4 107.8 %layer.1 = bf16[64,4096]{1,0:T(8,128)(2,1)} custom-call(bf16[256,256]{1,0:T(8,128)(2,1)} %q_one.1, bf16[256,256]{1,0:T(8,128)(2,1)} %q_two.1, bf16[256,128]{1,0:T(8,128)(2,1)} %k_one.1, bf16[256,128]{1,0:T(8,128)(2,1)} %k_two.1, bf16[256,256]{1,0:T(8,128)(2,1)} %val.1, f32[2]{0:T(128)} %lam.1, bf16[512,4096]{1,0:T(8,128)(2,1)} %w_out_h.1, ...), custom_call_target="tpu_custom_call" | custom-call | tf_op jit(solution)/shard_map/layer/pallas_call | solution.py:822
  109.2 1.9 %copy.22 = bf16[64,4096]{1,0:T(8,128)(2,1)} copy(bf16[64,4096]{1,0:T(8,128)(2,1)} %layer.1) | data formatting | bytes 1048576
where the time goes:
time: 111 us
  Pallas kernels  108 us (97%)
  local copies, waits for them, and re-layouts  2.57 us (2%)
    pallas_call x1, Pallas kernels, near(): pl.pallas_call(functools.partial(near_kernel, n, nt, group, pieces), out_...  108 us

commit v1 on v0

--- a/solution.py
+++ b/solution.py
@@ -230,27 +230,30 @@
     out,
     stacked, keys_one, keys_two, vals, peak, total, accum, rows_in,
     w, order, out_one, in_one, out_two, in_two, resid,
-    gates, ups, s_gate, s_up, wall, gathered, beside, out_hid, in_hid, out_sh, in_sh, units,
+    gates, ups, s_gate, s_up, wall, gathered, beside, stat, stat_b,
+    out_hid, in_hid, out_sh, in_sh, units, out_fin, in_fin, result,
     load, send_kv, recv_kv, send_one, recv_one, send_two, recv_two,
     send_g, recv_g, send_d, recv_d, send_sd, recv_sd,
     send_x, recv_x, send_b, recv_b, send_h, recv_h, send_s, recv_s,
+    send_u, recv_u, send_f, recv_f, save,
 ):
     me, mine = lax.axis_index("sp"), lax.axis_index("tp")
     place, side = me // 2, me % 2
     far, core = mine // 2, mine % 2
-    depth, half = n // 2, nt // 2
-    pair, partner = me + 1 - 2 * side, mine + 1 - 2 * core
+    depth = n // 2
+    pair, partner, across = me + 1 - 2 * side, mine + 1 - 2 * core, 2 * (1 - far) + core
     above, below = place < depth - 1, place > 0
     seq = q_one.shape[0]
     rows, width = stream.shape
     hid, wide = down_h.shape[0], s_down_h.shape[0]
     scale = HEAD ** (-0.5)
-
-    def fars(o):
-        return 2 * ((far + o) % half) + core
+    half = width // 2
 
     def column(o):
         return 2 * ((place + o) % depth) + side
+
+    def cols_of(f):
+        return pl.ds(pl.multiple_of(f * half, half), half)
 
     loads = [
         pltpu.make_async_copy(source, target, load.at[i])
@@ -261,18 +264,23 @@
                 (up_h, ups.at[0]),
                 (s_gate_h, s_gate),
                 (s_up_h, s_up),
-                (down_h, wall.at[pl.ds(pl.multiple_of(me * hid, hid), hid)]),
-                (s_down_h, wall.at[pl.ds(pl.multiple_of(n * hid + mine * wide, wide), wide)]),
+                (
+                    down_h.at[:, cols_of(far)],
+                    wall.at[pl.ds(pl.multiple_of(me * hid, hid), hid)],
+                ),
+                (
+                    s_down_h.at[:, cols_of(far)],
+                    wall.at[pl.ds(pl.multiple_of(n * hid + mine * wide, wide), wide)],
+                ),
             )
         )
     ]
     for o in range(1, depth):
         greet("sp", column(o))
     greet("sp", pair)
-    for o in range(1, half):
-        greet("tp", fars(o))
+    greet("tp", across)
     greet("tp", partner)
-    pl.semaphore_wait(pltpu.get_barrier_semaphore(), depth + half)
+    pl.semaphore_wait(pltpu.get_barrier_semaphore(), depth + 2)
 
     sources = (k_one, k_two, val)
     held = (keys_one, keys_two, vals)
@@ -323,13 +331,13 @@
     def down_at(block, c):
         return wall.at[pl.ds(pl.multiple_of(block * hid + c * part, part), part)]
 
-    def down_own(way, target, axis="sp"):
+    def down_own(way, target):
         return mesh_copy(
-            down_h.at[pl.ds(pl.multiple_of(core * part, part), part)],
+            down_h.at[pl.ds(pl.multiple_of(core * part, part), part), cols_of(far)],
             down_at(me, core),
             send_d.at[way],
             recv_d.at[0, me],
-            axis,
+            "sp",
             target,
         )
 
@@ -356,13 +364,13 @@
     def sd_at(u):
         return wall.at[pl.ds(pl.multiple_of(n * hid + u * wide, wide), wide)]
 
-    def sd_own(way, target):
-        return mesh_copy(s_down_h, sd_at(mine), send_sd.at[way], recv_sd.at[mine], "tp", target)
-
-    def sd_on(o, u):
+    def sd_own(way, f, target):
         return mesh_copy(
-            sd_at(u), sd_at(u), send_sd.at[half + o - 1], recv_sd.at[u], "tp", partner
-        )
+            s_down_h.at[:, cols_of(f)], sd_at(mine), send_sd.at[way], recv_sd.at[mine], "tp", target
+        )
+
+    def sd_on(u):
+        return mesh_copy(sd_at(u), sd_at(u), send_sd.at[2], recv_sd.at[u], "tp", partner)
 
     @pl.when(above)
     def _():
@@ -374,9 +382,13 @@
 
     for one in loads:
         one.start()
-    for o in range(1, half):
-        sd_own(o, fars(o)).start()
-    sd_own(0, partner).start()
+    late = place >= depth // 2
+
+    @pl.when(late)
+    def _():
+        sd_own(1, 1 - far, across).start()
+
+    sd_own(0, far, partner).start()
     for o in range(1, depth):
 
         @pl.when(place + o >= depth)
@@ -421,17 +433,22 @@
                 weights.astype(jnp.bfloat16), vals[block], preferred_element_type=jnp.float32
             )
 
+    def weights_out():
+        for one in pair_weights():
+            one.start()
+        down_own(0, pair).start()
+
+    pl.when(place == 0)(weights_out)
+
     def visit(e, carry):
         @pl.when(place >= e)
         def _():
             block = me - 2 * e
-            arrive(block)
-
-            @pl.when(above)
-            def _():
-                start(block, 0, me + 2)
-
-            start(block, 1, pair)
+            for up, over in zip(copies(block, 0, me + 2, False), copies(block, 1, pair, False)):
+                over.wait_recv()
+                pl.when(above)(up.start)
+                over.start()
+            pl.when(e == place)(weights_out)
             fold(block)
 
         @pl.when((place >= e - 1) & ((e > 1) | (side == 1)))
@@ -439,12 +456,6 @@
             block = pair - 2 * (e - 1)
             arrive(block)
             fold(block)
-
-        @pl.when(e == jnp.maximum(place, 1))
-        def _():
-            for one in pair_weights():
-                one.start()
-            down_own(0, pair).start()
 
         return carry
 
@@ -479,8 +490,8 @@
         size = head.shape[1]
         rows_in[:, h * size : (h + 1) * size] = head.astype(jnp.bfloat16)
 
-    for o in range(half):
-        base = 2 * ((far + o) % half)
+    for o in range(2):
+        base = 2 * ((far + o) % 2)
         for which, parity in enumerate((1 - core, core)):
             begin = pl.multiple_of((base + parity) * rows, rows)
             order[which, o * rows : (o + 1) * rows, :] = rows_in[pl.ds(begin, rows), :]
@@ -490,27 +501,17 @@
         for i in range(pieces)
     ]
     second = [
-        [
-            mesh_copy(
-                out_two.at[o, i],
-                in_two.at[o, i],
-                send_two.at[o, i],
-                recv_two.at[o, i],
-                "tp",
-                fars(o + 1),
-            )
-            for o in range(half - 1)
-        ]
+        mesh_copy(out_two.at[i], in_two.at[i], send_two.at[i], recv_two.at[i], "tp", across)
         for i in range(pieces)
     ]
     span = width // pieces
+    lift(1)
     loads[0].wait()
     for i in range(pieces):
         out_one[i] = jnp.dot(
             order[0], w[:, i * span : (i + 1) * span], preferred_element_type=jnp.float32
         ).astype(jnp.bfloat16)
         first[i].start()
-    lift(1)
     kept = []
     for i in range(pieces):
         sums = jnp.dot(
@@ -518,64 +519,82 @@
         )
         first[i].wait_recv()
         sums = sums + in_one[i].astype(jnp.float32)
-        for o in range(half - 1):
-            out_two[o, i] = sums[(o + 1) * rows : (o + 2) * rows].astype(jnp.bfloat16)
-            second[i][o].start()
+        out_two[i] = sums[rows:].astype(jnp.bfloat16)
+        second[i].start()
         kept.append(sums[:rows])
+
+    @pl.when(jnp.logical_not(late))
+    def _():
+        sd_own(1, 1 - far, across).start()
+
     for d in range(2, depth):
         lift(d)
-    for o in range(1, half):
-        u = fars(o)
-        sd_on(o, u).wait_recv()
-        sd_on(o, u).start()
+
+    def row_part(block, extra, spot, i):
+        return block.at[spot, i] if i < pieces else extra.at[spot]
+
+    def row_copy(spot, way, target, i):
+        some = row_part(gathered, stat, spot, i)
+        return mesh_copy(
+            some,
+            some,
+            send_x.at[way, i, spot],
+            recv_x.at[i, spot],
+            "sp",
+            target,
+        )
+
+    def beside_own(way, target, i):
+        return mesh_copy(
+            row_part(gathered, stat, place, i),
+            row_part(beside, stat_b, mine, i),
+            send_b.at[way, i],
+            recv_b.at[i, mine],
+            "tp",
+            target,
+        )
+
+    def beside_on(u, i):
+        some = row_part(beside, stat_b, u, i)
+        return mesh_copy(some, some, send_b.at[2, i], recv_b.at[i, u], "tp", partner)
+
+    def raise_row(e, i):
+        row_copy(place - e, 0, pair, i).wait_recv()
+        row_copy(place - e, 0, me + 2, i).start()
+
+    def lower_row(e, i):
+        row_copy(place + e, 0, pair, i).wait_recv()
+        row_copy(place + e, 1, me - 2, i).start()
+
+    def rows_out(i):
+        pl.when(above)(lambda: row_copy(place, 0, me + 2, i).start())
+        pl.when(below)(lambda: row_copy(place, 1, me - 2, i).start())
+        beside_own(1, across, i).start()
+        beside_own(0, partner, i).start()
+
+    fine = resid.shape[2]
+    per = span // fine
     squares = jnp.zeros((rows, 1), jnp.float32)
     for i in range(pieces):
         cut = slice(i * span, (i + 1) * span)
-        sums = kept[i]
-        for o in range(half - 1):
-            second[i][o].wait_recv()
-            sums = sums + in_two[o, i].astype(jnp.float32)
+        second[i].wait_recv()
+        sums = kept[i] + in_two[i].astype(jnp.float32)
         sums = (stream[:, cut].astype(jnp.float32) + sums).astype(jnp.bfloat16)
-        resid[:, cut] = sums
+        for j in range(per):
+            resid[i * per + j] = sums[:, j * fine : (j + 1) * fine]
         sums = sums.astype(jnp.float32)
         squares = squares + jnp.sum(sums * sums, axis=-1, keepdims=True)
+        gathered[place, i] = (sums * gain[:, cut]).astype(jnp.bfloat16)
+        rows_out(i)
     shrink = lax.rsqrt(squares / width + 1e-06)
-    for i in range(pieces):
-        cut = slice(i * span, (i + 1) * span)
-        gathered[place, :, cut] = (
-            resid[:, cut].astype(jnp.float32) * shrink * gain[:, cut]
-        ).astype(jnp.bfloat16)
-
-    chunk = rows // 2
-
-    def row_copy(spot, way, target, c):
-        some = gathered.at[spot, pl.ds(c * chunk, chunk)]
-        return mesh_copy(
-            some,
-            some,
-            send_x.at[way, c, spot],
-            recv_x.at[c, spot],
-            "sp",
-            target,
-        )
-
-    def beside_own(way, target):
-        return mesh_copy(
-            gathered.at[place], beside.at[mine], send_b.at[way], recv_b.at[mine], "tp", target
-        )
-
-    def beside_on(o, u):
-        return mesh_copy(
-            beside.at[u], beside.at[u], send_b.at[half + o - 1], recv_b.at[u], "tp", partner
-        )
-
-    for c in range(2):
-        pl.when(above)(lambda: row_copy(place, 0, me + 2, c).start())
-        pl.when(below)(lambda: row_copy(place, 1, me - 2, c).start())
-
-    for o in range(1, half):
-        beside_own(o, fars(o)).start()
-    beside_own(0, partner).start()
+    stat[place] = jnp.broadcast_to(shrink, stat.shape[1:])
+    rows_out(pieces)
+    for e in range(1, depth - 1):
+        for i in range(pieces + 1):
+            pl.when(above & (place >= e))(lambda: raise_row(e, i))
+            if e == depth - 2:
+                pl.when(above & below)(lambda: lower_row(1, i))
+
 
     def pass_down(e):
         def one(block, fresh):
@@ -594,19 +613,23 @@
         pl.when(place >= e)(lambda: one(pair - 2 * e))
         pl.when(place + e < depth)(lambda: one(pair + 2 * e))
 
-    for one, onward in zip(pair_weights(), pair_weights_on(share_at)):
-        one.wait_recv()
-        onward.start()
-    pass_down(1)
-    def hidden_of(block_rows, g, u):
-        gate_part = jnp.dot(block_rows, g, preferred_element_type=jnp.float32)
-        up_part = jnp.dot(block_rows, u, preferred_element_type=jnp.float32)
+    def hidden_of(block, spot, scales, g, u):
+        def project(m):
+            parts = [
+                jnp.dot(
+                    block[spot, i],
+                    m[i * span : (i + 1) * span, :],
+                    preferred_element_type=jnp.float32,
+                )
+                for i in range(pieces)
+            ]
+            return sum(parts[1:], parts[0]) * scales[spot][:, :1]
+
+        gate_part, up_part = project(g), project(u)
         return (gate_part / (1.0 + jnp.exp(-gate_part)) * up_part).astype(jnp.bfloat16)
 
     for i in range(1, 5):
         loads[i].wait()
-    in_sh[mine] = hidden_of(gathered[place], s_gate[...], s_up[...])
-    in_hid[place, side] = hidden_of(gathered[place], gates[0], ups[0])
 
     def hid_copy(spot):
         return mesh_copy(
@@ -615,8 +638,8 @@
         )
 
     def serve(spot):
-        out_hid[spot, side] = hidden_of(gathered[spot], gates[0], ups[0])
-        out_hid[spot, 1 - side] = hidden_of(gathered[spot], gates[1], ups[1])
+        out_hid[spot, side] = hidden_of(gathered, spot, stat, gates.at[0], ups.at[0])
+        out_hid[spot, 1 - side] = hidden_of(gathered, spot, stat, gates.at[1], ups.at[1])
         hid_copy(spot).start()
 
     def sh_copy(u):
@@ -625,23 +648,43 @@
         )
 
     def answer(u):
-        out_sh[u] = hidden_of(beside[u], s_gate[...], s_up[...])
+        out_sh[u] = hidden_of(beside, u, stat_b, s_gate, s_up)
         sh_copy(u).start()
 
     def turn(e, carry):
         low, high = place >= e, place + e < depth
 
-        for c in range(2):
-
-            @pl.when(low)
-            def _():
-                row_copy(place - e, 0, pair, c).wait_recv()
-                pl.when(above)(lambda: row_copy(place - e, 0, me + 2, c).start())
-
-            @pl.when(high)
-            def _():
-                row_copy(place + e, 0, pair, c).wait_recv()
-                pl.when(below)(lambda: row_copy(place + e, 1, me - 2, c).start())
+        @pl.when(low & jnp.logical_not(above))
+        def _():
+            for i in range(pieces + 1):
+                row_copy(place - e, 0, pair, i).wait_recv()
+
+        @pl.when(high)
+        def _():
+            for i in range(pieces + 1):
+                pl.when(below & (e > 1))(lambda: lower_row(e, i))
+                pl.when(jnp.logical_not(below))(
+                    lambda: row_copy(place + e, 0, pair, i).wait_recv()
+                )
+
+        @pl.when(e == 1)
+        def _():
+            for one, onward in zip(pair_weights(), pair_weights_on(share_at)):
+                one.wait_recv()
+                onward.start()
+            pass_down(1)
+            in_sh[mine] = hidden_of(gathered, place, stat, s_gate, s_up)
+            in_hid[place, side] = hidden_of(gathered, place, stat, gates.at[0], ups.at[0])
+            for one in pair_weights_on(other_at):
+                one.wait_recv()
+
+        @pl.when(low)
+        def _():
+            serve(place - e)
+
+        @pl.when(high)
+        def _():
+            serve(place + e)
 
         pass_down(e + 1)
 
@@ -649,62 +692,66 @@
         def _():
             down_pair(pair).wait_recv()
             down_core(pair, core).start()
-            for one in pair_weights_on(other_at):
-                one.wait_recv()
-
-        @pl.when(low)
-        def _():
-            serve(place - e)
-
-        @pl.when(high)
-        def _():
-            serve(place + e)
-
-        @pl.when(e > 1)
-        def _():
-            collect(e - 1)
-
-        @pl.when(e == 1)
-        def _():
-            in_hid[place, 1 - side] = hidden_of(gathered[place], gates[1], ups[1])
-            for o in range(1, half):
-                u = fars(o)
-                beside_on(o, u).wait_recv()
-                beside_on(o, u).start()
+            in_hid[place, 1 - side] = hidden_of(gathered, place, stat, gates.at[1], ups.at[1])
+            u = across
+            for i in range(pieces + 1):
+                beside_on(u, i).wait_recv()
+                beside_on(u, i).start()
+            answer(u)
+            sd_on(u).wait_recv()
+            sd_on(u).start()
+            for o in range(2):
+                u = 2 * ((far + o) % 2) + 1 - core
+                for i in range(pieces + 1):
+                    beside_on(u, i).wait_recv()
                 answer(u)
-            for o in range(half):
-                u = 2 * ((far + o) % half) + 1 - core
-                beside_on(1, u).wait_recv()
-                answer(u)
 
         return carry
 
     lax.fori_loop(1, depth, turn, 0)
 
-    collect(depth - 1)
-
-    for o in range(1, depth):
-        spot = (place + o) % depth
-        mesh_copy(
-            out_hid.at[spot], in_hid.at[spot], send_h.at[spot], recv_h.at[spot], "sp",
-            2 * spot + side,
-        ).wait_recv()
+    segments = units.shape[1]
+
+    def unit_copy(s):
+        return mesh_copy(
+            units.at[0, s], units.at[1, s], send_u.at[s], recv_u.at[s], "tp", across
+        )
+
     for o in range(1, nt):
         u = (mine + o) % nt
         mesh_copy(
             out_sh.at[u], in_sh.at[u], send_s.at[u], recv_s.at[u], "tp", u
         ).wait_recv()
-    for j in range(n):
-        units[:, j * hid : (j + 1) * hid] = (
-            in_hid[j // 2, j % 2].astype(jnp.float32) * mix[:, j : j + 1]
-        ).astype(jnp.bfloat16)
+    seg = units.shape[3]
     for j in range(nt):
-        units[:, n * hid + j * wide : n * hid + (j + 1) * wide] = in_sh[j]
+        at = j * wide
+        units[0, depth + at // seg, :, at % seg : at % seg + wide] = in_sh[j]
+    for s in range(depth, segments):
+        unit_copy(s).start()
+
+    for e in range(1, depth - 1):
+        collect(e)
+    for spot in range(depth):
+
+        @pl.when(place != spot)
+        def _():
+            mesh_copy(
+                out_hid.at[spot], in_hid.at[spot], send_h.at[spot], recv_h.at[spot], "sp",
+                2 * spot + side,
+            ).wait_recv()
+
+        for k in range(2):
+            j = 2 * spot + k
+            units[0, spot, :, k * hid : (k + 1) * hid] = (
+                in_hid[spot, k].astype(jnp.float32) * mix[:, j : j + 1]
+            ).astype(jnp.bfloat16)
+        unit_copy(spot).start()
+    collect(depth - 1)
 
     loads[5].wait()
     loads[6].wait()
-    for o in range(half):
-        sd_on(1, 2 * ((far + o) % half) + 1 - core).wait_recv()
+    for o in range(2):
+        sd_on(2 * ((far + o) % 2) + 1 - core).wait_recv()
 
     def receive_down(block, carry):
         @pl.when(block != me)
@@ -714,12 +761,43 @@
         return carry
 
     lax.fori_loop(0, n, receive_down, 0)
-    for i in range(2 * pieces):
-        cut = slice(i * span // 2, (i + 1) * span // 2)
-        out[:, cut] = (
-            resid[:, cut].astype(jnp.float32)
-            + jnp.dot(units[...], wall[:, cut], preferred_element_type=jnp.float32)
+    for s in range(segments):
+        unit_copy(s).wait_recv()
+
+    def fin_copy(i):
+        return mesh_copy(out_fin.at[i], in_fin.at[i], send_f.at[i], recv_f.at[i], "tp", across)
+
+    def put(spot):
+        return pltpu.make_async_copy(
+            result.at[spot],
+            out.at[:, pl.ds(pl.multiple_of(spot * fine, fine), fine)],
+            save.at[spot],
+        )
+
+    count = half // fine
+    for i in range(count):
+        cut = slice(i * fine, (i + 1) * fine)
+        terms = [
+            jnp.dot(
+                units[:, s].reshape(2 * rows, seg),
+                wall[s * seg : (s + 1) * seg, cut],
+                preferred_element_type=jnp.float32,
+            )
+            for s in range(segments)
+        ]
+        both = sum(terms[1:], terms[0])
+        out_fin[i] = both[rows:].astype(jnp.bfloat16)
+        fin_copy(i).start()
+        spot = far * count + i
+        result[spot] = (resid[spot].astype(jnp.float32) + both[:rows]).astype(jnp.bfloat16)
+        put(spot).start()
+    for i in range(count):
+        spot = (1 - far) * count + i
+        fin_copy(i).wait_recv()
+        result[spot] = (
+            resid[spot].astype(jnp.float32) + in_fin[i].astype(jnp.float32)
         ).astype(jnp.bfloat16)
+        put(spot).start()
 
     def settle(e, carry):
         @pl.when(place >= e)
@@ -730,8 +808,6 @@
             def _():
                 for one in copies(block, 0, me + 2, False):
                     one.wait_send()
-                for c in range(2):
-                    row_copy(place - e, 0, me + 2, c).wait_send()
 
                 @pl.when(e > 0)
                 def _():
@@ -744,8 +820,13 @@
 
         @pl.when((place + e < depth) & below)
         def _():
-            for c in range(2):
-                row_copy(place + e, 1, me - 2, c).wait_send()
+            for i in range(pieces + 1):
+                row_copy(place + e, 1, me - 2, i).wait_send()
+
+        @pl.when((place >= e) & above)
+        def _():
+            for i in range(pieces + 1):
+                row_copy(place - e, 0, me + 2, i).wait_send()
 
         @pl.when(e != place)
         def _():
@@ -764,25 +845,26 @@
         return carry
 
     lax.fori_loop(0, n, settle_down, 0)
-    for i in range(pieces):
-        first[i].wait_send()
-        for o in range(half - 1):
-            second[i][o].wait_send()
-    for one in pair_weights() + pair_weights_on(share_at):
+    for one in first + second + pair_weights() + pair_weights_on(share_at):
         one.wait_send()
     for o in range(1, depth):
         pl.when((place + o >= depth) | (o == 1))(lambda: down_own(o, column(o)).wait_send())
     down_own(0, pair).wait_send()
-    sd_own(0, partner).wait_send()
-    beside_own(0, partner).wait_send()
-    for o in range(1, half):
-        u = fars(o)
-        sd_own(o, u).wait_send()
-        sd_on(o, u).wait_send()
-        beside_own(o, u).wait_send()
-        beside_on(o, u).wait_send()
+    sd_own(0, far, partner).wait_send()
+    sd_own(1, 1 - far, across).wait_send()
+    sd_on(across).wait_send()
+    for i in range(pieces + 1):
+        beside_own(0, partner, i).wait_send()
+        beside_own(1, across, i).wait_send()
+        beside_on(across, i).wait_send()
     for o in range(1, nt):
         sh_copy((mine + o) % nt).wait_send()
+    for s in range(segments):
+        unit_copy(s).wait_send()
+    for i in range(count):
+        fin_copy(i).wait_send()
+    for i in range(2 * count):
+        put(i).wait()
 
 
 def near(
@@ -805,13 +887,16 @@
     s_down,
 ):
     n, nt = lax.axis_size("sp"), lax.axis_size("tp")
-    depth, half = n // 2, nt // 2
+    depth = n // 2
     seq, rows, width = q_first.shape[0], stream_in.shape[0], stream_in.shape[1]
     group, value_dim = q_first.shape[1] // HEAD, values.shape[1]
     hid, wide = w_down.shape[1], s_down.shape[0]
     tall, features = group * seq, group * value_dim
     pieces = 4
     span = width // pieces
+    half, fine = width // 2, width // 8
+    seg = 2 * hid
+    segments = depth + nt * wide // seg
     chosen = routes[:, :, None] == jnp.arange(n, dtype=jnp.int32)[None, None, :]
     mix = jnp.sum(jnp.where(chosen, route_w[:, :, None], 0.0), axis=1)
     vmem = pl.BlockSpec(memory_space=pltpu.VMEM)
@@ -823,7 +908,7 @@
         functools.partial(near_kernel, n, nt, group, pieces),
         out_shape=jax.ShapeDtypeStruct((rows, width), low),
         in_specs=[vmem] * 5 + [smem, hbm] + [vmem] * 3 + [hbm] * 6,
-        out_specs=vmem,
+        out_specs=hbm,
         scratch_shapes=[
             pltpu.VMEM((2, tall, HEAD), low),
             pltpu.VMEM((n, seq, HEAD), low),
@@ -834,45 +919,55 @@
             pltpu.VMEM((2, tall, value_dim), high),
             pltpu.VMEM((seq, features), low),
             pltpu.VMEM((features, width), low),
-            pltpu.VMEM((2, half * rows, features), low),
-            pltpu.VMEM((pieces, half * rows, span), low),
-            pltpu.VMEM((pieces, half * rows, span), low),
-            pltpu.VMEM((half - 1, pieces, rows, span), low),
-            pltpu.VMEM((half - 1, pieces, rows, span), low),
-            pltpu.VMEM((rows, width), low),
+            pltpu.VMEM((2, 2 * rows, features), low),
+            pltpu.VMEM((pieces, 2 * rows, span), low),
+            pltpu.VMEM((pieces, 2 * rows, span), low),
+            pltpu.VMEM((pieces, rows, span), low),
+            pltpu.VMEM((pieces, rows, span), low),
+            pltpu.VMEM((width // fine, rows, fine), low),
             pltpu.VMEM((2, width, hid), low),
             pltpu.VMEM((2, width, hid), low),
             pltpu.VMEM((width, wide), low),
             pltpu.VMEM((width, wide), low),
-            pltpu.VMEM((n * hid + nt * wide, width), low),
-            pltpu.VMEM((depth, rows, width), low),
-            pltpu.VMEM((nt, rows, width), low),
+            pltpu.VMEM((n * hid + nt * wide, half), low),
+            pltpu.VMEM((depth, pieces, rows, span), low),
+            pltpu.VMEM((nt, pieces, rows, span), low),
+            pltpu.VMEM((depth, rows, HEAD), high),
+            pltpu.VMEM((nt, rows, HEAD), high),
             pltpu.VMEM((depth, 2, rows, hid), low),
             pltpu.VMEM((depth, 2, rows, hid), low),
             pltpu.VMEM((nt, rows, wide), low),
             pltpu.VMEM((nt, rows, wide), low),
-            pltpu.VMEM((rows, n * hid + nt * wide), low),
+            pltpu.VMEM((2, segments, rows, seg), low),
+            pltpu.VMEM((half // fine, rows, fine), low),
+            pltpu.VMEM((half // fine, rows, fine), low),
+            pltpu.VMEM((width // fine, rows, fine), low),
             dma((7,)),
             dma((2, 3, n)),
             dma((3, n)),
             dma((pieces,)),
             dma((pieces,)),
-            dma((half - 1, pieces)),
-            dma((half - 1, pieces)),
+            dma((pieces,)),
+            dma((pieces,)),
             dma((2, 2)),
             dma((2, 2)),
             dma((depth + 3 * n,)),
             dma((2, n)),
+            dma((3,)),
             dma((nt,)),
-            dma((nt,)),
-            dma((2, 2, depth)),
-            dma((2, depth)),
-            dma((nt,)),
-            dma((nt,)),
+            dma((2, pieces + 1, depth)),
+            dma((pieces + 1, depth)),
+            dma((3, pieces + 1)),
+            dma((pieces + 1, nt)),
             dma((depth,)),
             dma((depth,)),
             dma((nt,)),
             dma((nt,)),
+            dma((segments,)),
+            dma((segments,)),
+            dma((half // fine,)),
+            dma((half // fine,)),
+            dma((width // fine,)),
         ],
         compiler_params=pltpu.CompilerParams(
             collective_id=0, has_side_effects=True, vmem_limit_bytes=60 << 20
@@ -888,14 +983,17 @@
     n, nt = lax.axis_size("sp"), lax.axis_size("tp")
     k_first, values, w_gate, w_down, s_down = (arrays[i] for i in (3, 5, 11, 13, 16))
     fits = (
-        2 <= n <= 16
+        4 <= n <= 16
         and n % 2 == 0
-        and nt >= 4
-        and nt % 2 == 0
+        and nt == 4
         and k_first.shape[1] == HEAD
         and w_gate.shape[0] == 1
         and w_down.shape[1] % (16 * nt) == 0
         and s_down.shape[0] % (16 * n) == 0
+        and w_down.shape[1] % HEAD == 0
+        and (2 * w_down.shape[1]) % s_down.shape[0] == 0
+        and (nt * s_down.shape[0]) % (2 * w_down.shape[1]) == 0
+        and w_down.shape[2] % (16 * HEAD) == 0
     )
     return near(*arrays) if fits else local(*arrays)
 

time: 111 us -> 102 us (0.919)
  Pallas kernels: 108 us -> 98.8 us
    pallas_call x1, Pallas kernels: 108 us -> 98.8 us  [near(): pl.pallas_call(functools.partial(near_kernel, n, nt, group, pieces), out_...]
where the time goes in v1:
time: 102 us
  Pallas kernels  98.8 us (97%)
  local copies, waits for them, and re-layouts  2.57 us (3%)
    pallas_call x1, Pallas kernels, near(): pl.pallas_call(functools.partial(near_kernel, n, nt, group, pieces), out_...  98.8 us

profile of v1, /device:TPU:0, one launch (start us, length us, event | category | flops | bytes accessed | tf_op | source)
XLA Modules:
  0.0 102.0 jit_solution(13969563460805401181)
XLA Ops:
  0.0 0.7 select_reduce_fusion
  0.7 0.7 copy.20.mix
  1.4 98.8 %layer.1 = bf16[64,4096]{1,0:T(8,128)(2,1)} custom-call(bf16[256,256]{1,0:T(8,128)(2,1)} %q_one.1, bf16[256,256]{1,0:T(8,128)(2,1)} %q_two.1, bf16[256,128]{1,0:T(8,128)(2,1)} %k_one.1, bf16[256,128]{1,0:T(8,128)(2,1)} %k_two.1, bf16[256,256]{1,0:T(8,128)(2,1)} %val.1, f32[2]{0:T(128)} %lam.1, bf16[512,4096]{1,0:T(8,128)(2,1)} %w_out_h.1, ...), custom_call_target="tpu_custom_call" | custom-call | tf_op jit(solution)/shard_map/layer/pallas_call | solution.py:907
  100.2 1.9 %copy.22 = bf16[64,4096]{1,0:T(8,128)(2,1)} copy(bf16[64,4096]{1,0:T(8,128)(2,1)} %layer.1) | data formatting | bytes 1048576

commit v2 on v1

--- a/solution.py
+++ b/solution.py
@@ -225,17 +225,18 @@
 
 def near_kernel(
     n, nt, group, pieces,
-    q_one, q_two, k_one, k_two, val, lam, w_out_h, stream, gain, mix,
+    q_one_h, q_two_h, k_one_h, k_two_h, val_h, lam, w_out_h, stream_h, gain_h, mix_h,
     gate_h, up_h, s_gate_h, s_up_h, down_h, s_down_h,
     out,
+    q_one, q_two, k_one, k_two, val, stream, gain, mix_t,
     stacked, keys_one, keys_two, vals, peak, total, accum, rows_in,
     w, order, out_one, in_one, out_two, in_two, resid,
     gates, ups, s_gate, s_up, wall, gathered, beside, stat, stat_b,
-    out_hid, in_hid, out_sh, in_sh, units, out_fin, in_fin, result,
+    out_hid, in_hid, out_sh, in_sh, units, out_fin, in_fin, result, mix, square, extra, partial,
     load, send_kv, recv_kv, send_one, recv_one, send_two, recv_two,
     send_g, recv_g, send_d, recv_d, send_sd, recv_sd,
     send_x, recv_x, send_b, recv_b, send_h, recv_h, send_s, recv_s,
-    send_u, recv_u, send_f, recv_f, save,
+    send_u, recv_u, send_f, recv_f, save, send_e, recv_e,
 ):
     me, mine = lax.axis_index("sp"), lax.axis_index("tp")
     place, side = me // 2, me % 2
@@ -280,6 +281,25 @@
     greet("sp", pair)
     greet("tp", across)
     greet("tp", partner)
+    inputs = [
+        pltpu.make_async_copy(source, target, load.at[7 + i])
+        for i, (source, target) in enumerate(
+            (
+                (k_one_h, k_one),
+                (k_two_h, k_two),
+                (val_h, val),
+                (q_one_h, q_one),
+                (q_two_h, q_two),
+                (stream_h, stream),
+                (gain_h, gain),
+                (mix_h, mix_t),
+            )
+        )
+    ]
+    for one in inputs:
+        one.start()
+    for one in inputs[:3]:
+        one.wait()
     pl.semaphore_wait(pltpu.get_barrier_semaphore(), depth + 2)
 
     sources = (k_one, k_two, val)
@@ -290,7 +310,7 @@
             mesh_copy(
                 sources[a] if own else held[a].at[block],
                 held[a].at[block],
-                send_kv.at[way, a, block],
+                send_kv.at[way, a, block // 2],
                 recv_kv.at[a, block],
                 "sp",
                 target,
@@ -345,7 +365,7 @@
         return mesh_copy(
             down_at(block, core),
             down_at(block, core),
-            send_d.at[depth + block],
+            send_d.at[depth + block // 2],
             recv_d.at[0, block],
             "sp",
             pair,
@@ -355,12 +375,35 @@
         return mesh_copy(
             down_at(block, c),
             down_at(block, c),
-            send_d.at[depth + n + block],
+            send_d.at[3 * depth + block],
             recv_d.at[1, block],
             "tp",
             partner,
         )
 
+    def extra_at(s, c):
+        return extra.at[pl.ds(pl.multiple_of(s * hid + c * part, part), part)]
+
+    def extra_own():
+        return mesh_copy(
+            down_h.at[pl.ds(pl.multiple_of(core * part, part), part), cols_of(1 - far)],
+            extra_at(side, core),
+            send_e.at[0],
+            recv_e.at[0, side],
+            "sp",
+            side,
+        )
+
+    def extra_pair(s):
+        return mesh_copy(
+            extra_at(s, core), extra_at(s, core), send_e.at[1], recv_e.at[0, s], "sp", pair
+        )
+
+    def extra_core(s, c):
+        return mesh_copy(
+            extra_at(s, c), extra_at(s, c), send_e.at[2 + s], recv_e.at[1, s], "tp", partner
+        )
+
     def sd_at(u):
         return wall.at[pl.ds(pl.multiple_of(n * hid + u * wide, wide), wide)]
 
@@ -395,6 +438,11 @@
         def _():
             down_own(o, column(o)).start()
 
+    top_place = place == depth - 1
+    pl.when(top_place)(lambda: extra_own().start())
+
+    for one in inputs[3:]:
+        one.wait()
     for index, q in enumerate((q_one, q_two)):
         for h in range(group):
             stacked[index, h * seq : (h + 1) * seq, :] = q[:, h * HEAD : (h + 1) * HEAD]
@@ -433,10 +481,28 @@
                 weights.astype(jnp.bfloat16), vals[block], preferred_element_type=jnp.float32
             )
 
+    def down_up(block):
+        return mesh_copy(
+            down_at(block, core),
+            down_at(block, core),
+            send_d.at[2 * depth + block // 2],
+            recv_d.at[0, block],
+            "sp",
+            me + 2,
+        )
+
+    def lift(d):
+        @pl.when((place >= d) & above)
+        def _():
+            down_up(me - 2 * d).wait_recv()
+            down_up(me - 2 * d).start()
+
     def weights_out():
+        pl.when(above)(lambda: down_own(1, me + 2).start())
         for one in pair_weights():
             one.start()
         down_own(0, pair).start()
+        lift(1)
 
     pl.when(place == 0)(weights_out)
 
@@ -461,25 +527,8 @@
 
     lax.fori_loop(1, depth + 1, visit, 0)
 
-    @pl.when(above)
-    def _():
-        down_own(1, me + 2).start()
-
-    def down_up(block):
-        return mesh_copy(
-            down_at(block, core),
-            down_at(block, core),
-            send_d.at[depth + 2 * n + block],
-            recv_d.at[0, block],
-            "sp",
-            me + 2,
-        )
-
-    def lift(d):
-        @pl.when((place >= d) & above)
-        def _():
-            down_up(me - 2 * d).wait_recv()
-            down_up(me - 2 * d).start()
+    for d in range(2, depth):
+        lift(d)
 
     for h in range(group):
         cut = slice(h * seq, (h + 1) * seq)
@@ -497,15 +546,14 @@
             order[which, o * rows : (o + 1) * rows, :] = rows_in[pl.ds(begin, rows), :]
 
     first = [
-        mesh_copy(out_one.at[i], in_one.at[i], send_one.at[i], recv_one.at[i], "tp", partner)
+        mesh_copy(out_one.at[i], in_one.at[i], send_one.at[0], recv_one.at[i], "tp", partner)
         for i in range(pieces)
     ]
     second = [
-        mesh_copy(out_two.at[i], in_two.at[i], send_two.at[i], recv_two.at[i], "tp", across)
+        mesh_copy(out_two.at[i], in_two.at[i], send_two.at[0], recv_two.at[i], "tp", across)
         for i in range(pieces)
     ]
     span = width // pieces
-    lift(1)
     loads[0].wait()
     for i in range(pieces):
         out_one[i] = jnp.dot(
@@ -527,9 +575,6 @@
     def _():
         sd_own(1, 1 - far, across).start()
 
-    for d in range(2, depth):
-        lift(d)
-
     def row_part(block, extra, spot, i):
         return block.at[spot, i] if i < pieces else extra.at[spot]
 
@@ -538,25 +583,31 @@
         return mesh_copy(
             some,
             some,
-            send_x.at[way, i, spot],
+            send_x.at[way, i // pieces, spot],
             recv_x.at[i, spot],
             "sp",
             target,
         )
 
+    def rows_sent(spot, way):
+        for some, kind in ((gathered.at[spot], 0), (stat.at[spot], 1)):
+            mesh_copy(
+                some, some, send_x.at[way, kind, spot], recv_x.at[0, spot], "sp", pair
+            ).wait_send()
+
     def beside_own(way, target, i):
         return mesh_copy(
             row_part(gathered, stat, place, i),
             row_part(beside, stat_b, mine, i),
-            send_b.at[way, i],
-            recv_b.at[i, mine],
+            send_b.at[way, i // pieces],
+            recv_b.at[i // pieces, mine],
             "tp",
             target,
         )
 
-    def beside_on(u, i):
-        some = row_part(beside, stat_b, u, i)
-        return mesh_copy(some, some, send_b.at[2, i], recv_b.at[i, u], "tp", partner)
+    def beside_on(u, kind, way=2):
+        some = (beside, stat_b)[kind].at[u]
+        return mesh_copy(some, some, send_b.at[way, kind], recv_b.at[kind, u], "tp", partner)
 
     def raise_row(e, i):
         row_copy(place - e, 0, pair, i).wait_recv()
@@ -628,6 +679,11 @@
         gate_part, up_part = project(g), project(u)
         return (gate_part / (1.0 + jnp.exp(-gate_part)) * up_part).astype(jnp.bfloat16)
 
+    square[...] = jnp.zeros_like(square)
+    square[0:n, 0:rows] = mix_t[...]
+    turned = square[...].T
+    for j in range(n):
+        mix[j] = jnp.broadcast_to(turned[0:rows, j : j + 1], mix.shape[1:])
     for i in range(1, 5):
         loads[i].wait()
 
@@ -688,27 +744,40 @@
 
         pass_down(e + 1)
 
-        @pl.when(e == 1)
+        @pl.when(e == 2)
         def _():
             down_pair(pair).wait_recv()
             down_core(pair, core).start()
             in_hid[place, 1 - side] = hidden_of(gathered, place, stat, gates.at[1], ups.at[1])
             u = across
-            for i in range(pieces + 1):
-                beside_on(u, i).wait_recv()
-                beside_on(u, i).start()
+            for kind in range(2):
+                beside_on(u, kind).wait_recv()
+                beside_on(u, kind).start()
             answer(u)
             sd_on(u).wait_recv()
             sd_on(u).start()
             for o in range(2):
                 u = 2 * ((far + o) % 2) + 1 - core
-                for i in range(pieces + 1):
-                    beside_on(u, i).wait_recv()
+                for kind in range(2):
+                    beside_on(u, kind).wait_recv()
                 answer(u)
 
         return carry
 
-    lax.fori_loop(1, depth, turn, 0)
+    @pl.when(place == 0)
+    def _():
+        extra_pair(side).wait_recv()
+        extra_pair(side).start()
+        extra_core(side, core).start()
+
+    lax.fori_loop(1, depth - 1, turn, 0)
+    last = depth - 1
+
+    @pl.when(place == 0)
+    def _():
+        for i in range(pieces + 1):
+            row_copy(last, 0, pair, i).wait_recv()
+        serve(last)
 
     segments = units.shape[1]
 
@@ -731,8 +800,8 @@
 
     for e in range(1, depth - 1):
         collect(e)
-    for spot in range(depth):
-
+
+    def place_unit(spot):
         @pl.when(place != spot)
         def _():
             mesh_copy(
@@ -743,10 +812,30 @@
         for k in range(2):
             j = 2 * spot + k
             units[0, spot, :, k * hid : (k + 1) * hid] = (
-                in_hid[spot, k].astype(jnp.float32) * mix[:, j : j + 1]
+                in_hid[spot, k].astype(jnp.float32) * mix[j][:, :1]
             ).astype(jnp.bfloat16)
+
+    for spot in range(last - 1, -1, -1):
+        place_unit(spot)
         unit_copy(spot).start()
-    collect(depth - 1)
+
+    @pl.when(place != 0)
+    def _():
+        place_unit(last)
+        unit_copy(last).start()
+
+    @pl.when(top_place)
+    def _():
+        for i in range(pieces + 1):
+            row_copy(0, 0, pair, i).wait_recv()
+        serve(0)
+
+    @pl.when(place == 0)
+    def _():
+        extra_pair(1 - side).wait_recv()
+        extra_core(1 - side, core).start()
+
+    collect(last)
 
     loads[5].wait()
     loads[6].wait()
@@ -761,11 +850,12 @@
         return carry
 
     lax.fori_loop(0, n, receive_down, 0)
-    for s in range(segments):
+    early = [s for s in range(segments) if s != last]
+    for s in early:
         unit_copy(s).wait_recv()
 
     def fin_copy(i):
-        return mesh_copy(out_fin.at[i], in_fin.at[i], send_f.at[i], recv_f.at[i], "tp", across)
+        return mesh_copy(out_fin.at[i], in_fin.at[i], send_f.at[0], recv_f.at[i], "tp", across)
 
     def put(spot):
         return pltpu.make_async_copy(
@@ -775,6 +865,7 @@
         )
 
     count = half // fine
+    mine_at, other_of = far * count, (1 - far) * count
     for i in range(count):
         cut = slice(i * fine, (i + 1) * fine)
         terms = [
@@ -783,21 +874,53 @@
                 wall[s * seg : (s + 1) * seg, cut],
                 preferred_element_type=jnp.float32,
             )
-            for s in range(segments)
+            for s in early
         ]
         both = sum(terms[1:], terms[0])
-        out_fin[i] = both[rows:].astype(jnp.bfloat16)
-        fin_copy(i).start()
-        spot = far * count + i
-        result[spot] = (resid[spot].astype(jnp.float32) + both[:rows]).astype(jnp.bfloat16)
+        partial[i] = both
+
+        @pl.when(place == 0)
+        def _():
+            out_fin[i] = both[rows:].astype(jnp.bfloat16)
+            fin_copy(i).start()
+
+    def close(spot, terms):
+        result[spot] = (resid[spot].astype(jnp.float32) + terms).astype(jnp.bfloat16)
         put(spot).start()
-    for i in range(count):
-        spot = (1 - far) * count + i
-        fin_copy(i).wait_recv()
-        result[spot] = (
-            resid[spot].astype(jnp.float32) + in_fin[i].astype(jnp.float32)
-        ).astype(jnp.bfloat16)
-        put(spot).start()
+
+    @pl.when(place == 0)
+    def _():
+        extra_core(0, 1 - core).wait_recv()
+        extra_core(1, 1 - core).wait_recv()
+        for i in range(count):
+            fin_copy(i).wait_recv()
+        place_unit(last)
+        rest = units[0, last]
+        for i in range(count):
+            cut = slice(i * fine, (i + 1) * fine)
+            terms = jnp.dot(
+                rest, wall[last * seg : (last + 1) * seg, cut], preferred_element_type=jnp.float32
+            )
+            close(mine_at + i, partial[i, :rows] + terms)
+            terms = jnp.dot(rest, extra[:, cut], preferred_element_type=jnp.float32)
+            close(other_of + i, in_fin[i].astype(jnp.float32) + terms)
+
+    @pl.when(place != 0)
+    def _():
+        unit_copy(last).wait_recv()
+        for i in range(count):
+            cut = slice(i * fine, (i + 1) * fine)
+            both = partial[i] + jnp.dot(
+                units[:, last].reshape(2 * rows, seg),
+                wall[last * seg : (last + 1) * seg, cut],
+                preferred_element_type=jnp.float32,
+            )
+            out_fin[i] = both[rows:].astype(jnp.bfloat16)
+            fin_copy(i).start()
+            close(mine_at + i, both[:rows])
+        for i in range(count):
+            fin_copy(i).wait_recv()
+            close(other_of + i, in_fin[i].astype(jnp.float32))
 
     def settle(e, carry):
         @pl.when(place >= e)
@@ -818,15 +941,8 @@
                 for one in copies(block, 1, pair, False):
                     one.wait_send()
 
-        @pl.when((place + e < depth) & below)
-        def _():
-            for i in range(pieces + 1):
-                row_copy(place + e, 1, me - 2, i).wait_send()
-
-        @pl.when((place >= e) & above)
-        def _():
-            for i in range(pieces + 1):
-                row_copy(place - e, 0, me + 2, i).wait_send()
+        pl.when((place + e < depth) & below)(lambda: rows_sent(place + e, 1))
+        pl.when((place >= e) & above)(lambda: rows_sent(place - e, 0))
 
         @pl.when(e != place)
         def _():
@@ -845,24 +961,36 @@
         return carry
 
     lax.fori_loop(0, n, settle_down, 0)
-    for one in first + second + pair_weights() + pair_weights_on(share_at):
+    for one in pair_weights() + pair_weights_on(share_at):
         one.wait_send()
+    for some, sem, rec in (
+        (out_one, send_one.at[0], recv_one.at[0]),
+        (out_two, send_two.at[0], recv_two.at[0]),
+        (out_fin, send_f.at[0], recv_f.at[0]),
+    ):
+        mesh_copy(some, some, sem, rec, "tp", partner).wait_send()
     for o in range(1, depth):
         pl.when((place + o >= depth) | (o == 1))(lambda: down_own(o, column(o)).wait_send())
     down_own(0, pair).wait_send()
     sd_own(0, far, partner).wait_send()
     sd_own(1, 1 - far, across).wait_send()
     sd_on(across).wait_send()
-    for i in range(pieces + 1):
-        beside_own(0, partner, i).wait_send()
-        beside_own(1, across, i).wait_send()
-        beside_on(across, i).wait_send()
+    for kind in range(2):
+        for way in range(3):
+            beside_on(across, kind, way).wait_send()
     for o in range(1, nt):
         sh_copy((mine + o) % nt).wait_send()
-    for s in range(segments):
+    for s in early:
         unit_copy(s).wait_send()
-    for i in range(count):
-        fin_copy(i).wait_send()
+    pl.when(place != 0)(lambda: unit_copy(last).wait_send())
+    pl.when(top_place)(lambda: extra_own().wait_send())
+
+    @pl.when(place == 0)
+    def _():
+        extra_pair(side).wait_send()
+        extra_core(0, core).wait_send()
+        extra_core(1, core).wait_send()
+
     for i in range(2 * count):
         put(i).wait()
 
@@ -897,9 +1025,8 @@
     half, fine = width // 2, width // 8
     seg = 2 * hid
     segments = depth + nt * wide // seg
-    chosen = routes[:, :, None] == jnp.arange(n, dtype=jnp.int32)[None, None, :]
-    mix = jnp.sum(jnp.where(chosen, route_w[:, :, None], 0.0), axis=1)
-    vmem = pl.BlockSpec(memory_space=pltpu.VMEM)
+    chosen = routes.T[None, :, :] == jnp.arange(n, dtype=jnp.int32)[:, None, None]
+    mix_t = jnp.sum(jnp.where(chosen, route_w.T[None, :, :], 0.0), axis=1)
     smem = pl.BlockSpec(memory_space=pltpu.SMEM)
     hbm = pl.BlockSpec(memory_space=pl.ANY)
     low, high = jnp.bfloat16, jnp.float32
@@ -907,9 +1034,17 @@
     return pl.pallas_call(
         functools.partial(near_kernel, n, nt, group, pieces),
         out_shape=jax.ShapeDtypeStruct((rows, width), low),
-        in_specs=[vmem] * 5 + [smem, hbm] + [vmem] * 3 + [hbm] * 6,
+        in_specs=[hbm] * 5 + [smem] + [hbm] * 10,
         out_specs=hbm,
         scratch_shapes=[
+            pltpu.VMEM((seq, group * HEAD), low),
+            pltpu.VMEM((seq, group * HEAD), low),
+            pltpu.VMEM((seq, HEAD), low),
+            pltpu.VMEM((seq, HEAD), low),
+            pltpu.VMEM((seq, value_dim), low),
+            pltpu.VMEM((rows, width), low),
+            pltpu.VMEM((1, width), high),
+            pltpu.VMEM((n, rows), high),
             pltpu.VMEM((2, tall, HEAD), low),
             pltpu.VMEM((n, seq, HEAD), low),
             pltpu.VMEM((n, seq, HEAD), low),
@@ -942,32 +1077,38 @@
             pltpu.VMEM((half // fine, rows, fine), low),
             pltpu.VMEM((half // fine, rows, fine), low),
             pltpu.VMEM((width // fine, rows, fine), low),
-            dma((7,)),
-            dma((2, 3, n)),
+            pltpu.VMEM((n, rows, HEAD), high),
+            pltpu.VMEM((HEAD, HEAD), high),
+            pltpu.VMEM((2 * hid, half), low),
+            pltpu.VMEM((half // fine, 2 * rows, fine), high),
+            dma((15,)),
+            dma((2, 3, depth)),
             dma((3, n)),
+            dma((1,)),
             dma((pieces,)),
-            dma((pieces,)),
-            dma((pieces,)),
+            dma((1,)),
             dma((pieces,)),
             dma((2, 2)),
             dma((2, 2)),
-            dma((depth + 3 * n,)),
+            dma((3 * depth + n,)),
             dma((2, n)),
             dma((3,)),
             dma((nt,)),
-            dma((2, pieces + 1, depth)),
+            dma((2, 2, depth)),
             dma((pieces + 1, depth)),
-            dma((3, pieces + 1)),
-            dma((pieces + 1, nt)),
+            dma((3, 2)),
+            dma((2, nt)),
             dma((depth,)),
             dma((depth,)),
             dma((nt,)),
             dma((nt,)),
             dma((segments,)),
             dma((segments,)),
-            dma((half // fine,)),
+            dma((1,)),
             dma((half // fine,)),
             dma((width // fine,)),
+            dma((4,)),
+            dma((2, 2)),
         ],
         compiler_params=pltpu.CompilerParams(
             collective_id=0, has_side_effects=True, vmem_limit_bytes=60 << 20
@@ -975,7 +1116,7 @@
         name="layer",
     )(
         q_first, q_second, k_first, k_second, values, head_lambda, w_out, stream_in,
-        norm_gain.reshape(1, width), mix, w_gate[0], w_up[0], s_gate, s_up, w_down[0], s_down,
+        norm_gain.reshape(1, width), mix_t, w_gate[0], w_up[0], s_gate, s_up, w_down[0], s_down,
     )
 
 
@@ -987,6 +1128,7 @@
         and n % 2 == 0
         and nt == 4
         and k_first.shape[1] == HEAD
+        and arrays[0].shape[0] <= HEAD
         and w_gate.shape[0] == 1
         and w_down.shape[1] % (16 * nt) == 0
         and s_down.shape[0] % (16 * n) == 0

time: 102 us -> 93.5 us (0.917); the launches traced: 102 us -> 92.2 us
  Pallas kernels: 98.8 us -> 89 us
    pallas_call x1, Pallas kernels: 98.8 us -> 89 us  [near(): pl.pallas_call(functools.partial(near_kernel, n, nt, group, pieces), out_...]
where the time goes in v2:
time: 93.5 us; the launch traced here: 92.2 us
  Pallas kernels  89 us (95%)
  local copies, waits for them, and re-layouts  1.87 us (2%)
  other arithmetic  1.3 us (1%)
    pallas_call x1, Pallas kernels, near(): pl.pallas_call(functools.partial(near_kernel, n, nt, group, pieces), out_...  89 us

profile of v2, /device:TPU:0, one launch (start us, length us, event | category | flops | bytes accessed | tf_op | source)
XLA Modules:
  0.0 92.2 jit_solution(7773853186693442007)
XLA Ops:
  0.0 1.3 %select_reduce_fusion.mix_h = f32[8,64]{1,0:T(8,128)} fusion(f32[4,64]{1,0:T(4,128)} %bitcast.10, s32[4,64]{1,0:T(4,128)} %bitcast.11), kind=kLoop, calls=%fused_computation | loop fusion | flops 5632 | bytes 4096 | tf_op jit(solution)/shard_map/reduce_sum | solution.py:1029
  1.3 89.0 %layer.1 = bf16[64,4096]{1,0:T(8,128)(2,1)} custom-call(bf16[256,256]{1,0:T(8,128)(2,1)} %q_one_h.1, bf16[256,256]{1,0:T(8,128)(2,1)} %q_two_h.1, bf16[256,128]{1,0:T(8,128)(2,1)} %k_one_h.1, bf16[256,128]{1,0:T(8,128)(2,1)} %k_two_h.1, bf16[256,256]{1,0:T(8,128)(2,1)} %val_h.1, f32[2]{0:T(128)} %lam.1, bf16[512,4096]{1,0:T(8,128)(2,1)} %w_out_h.1, ...), custom_call_target="tpu_custom_call" | custom-call | tf_op jit(solution)/shard_map/layer/pallas_call | solution.py:1034
  90.3 1.9 %copy.19 = bf16[64,4096]{1,0:T(8,128)(2,1)} copy(bf16[64,4096]{1,0:T(8,128)(2,1)} %layer.1) | data formatting | bytes 1048576

commit v3 on v2

--- a/solution.py
+++ b/solution.py
@@ -225,10 +225,10 @@
 
 def near_kernel(
     n, nt, group, pieces,
-    q_one_h, q_two_h, k_one_h, k_two_h, val_h, lam, w_out_h, stream_h, gain_h, mix_h,
+    q_one_h, q_two_h, k_one_h, k_two_h, val_h, lam, w_out_h, stream_h, gain_h, route_h, share_h,
     gate_h, up_h, s_gate_h, s_up_h, down_h, s_down_h,
     out,
-    q_one, q_two, k_one, k_two, val, stream, gain, mix_t,
+    q_one, q_two, k_one, k_two, val, stream, gain, route_t, share_t,
     stacked, keys_one, keys_two, vals, peak, total, accum, rows_in,
     w, order, out_one, in_one, out_two, in_two, resid,
     gates, ups, s_gate, s_up, wall, gathered, beside, stat, stat_b,
@@ -292,7 +292,8 @@
                 (q_two_h, q_two),
                 (stream_h, stream),
                 (gain_h, gain),
-                (mix_h, mix_t),
+                (route_h, route_t),
+                (share_h, share_t),
             )
         )
     ]
@@ -638,7 +639,8 @@
         gathered[place, i] = (sums * gain[:, cut]).astype(jnp.bfloat16)
         rows_out(i)
     shrink = lax.rsqrt(squares / width + 1e-06)
-    stat[place] = jnp.broadcast_to(shrink, stat.shape[1:])
+    square[0:rows, :] = jnp.broadcast_to(shrink, (rows, HEAD))
+    stat[place] = square[...].T[0 : stat.shape[1], :]
     rows_out(pieces)
     for e in range(1, depth - 1):
         for i in range(pieces + 1):
@@ -664,7 +666,11 @@
         pl.when(place >= e)(lambda: one(pair - 2 * e))
         pl.when(place + e < depth)(lambda: one(pair + 2 * e))
 
-    def hidden_of(block, spot, scales, g, u):
+    def factors(scales, spot):
+        square[0 : scales.shape[1], :] = scales[spot]
+        return square[...].T[0:rows, :1]
+
+    def hidden_of(block, spot, factor, g, u):
         def project(m):
             parts = [
                 jnp.dot(
@@ -674,13 +680,15 @@
                 )
                 for i in range(pieces)
             ]
-            return sum(parts[1:], parts[0]) * scales[spot][:, :1]
+            return sum(parts[1:], parts[0]) * factor
 
         gate_part, up_part = project(g), project(u)
         return (gate_part / (1.0 + jnp.exp(-gate_part)) * up_part).astype(jnp.bfloat16)
 
     square[...] = jnp.zeros_like(square)
-    square[0:n, 0:rows] = mix_t[...]
+    for j in range(n):
+        chosen = jnp.where(route_t[...] == j, share_t[...], 0.0)
+        square[j : j + 1, 0:rows] = jnp.sum(chosen, axis=0, keepdims=True)
     turned = square[...].T
     for j in range(n):
         mix[j] = jnp.broadcast_to(turned[0:rows, j : j + 1], mix.shape[1:])
@@ -694,8 +702,9 @@
         )
 
     def serve(spot):
-        out_hid[spot, side] = hidden_of(gathered, spot, stat, gates.at[0], ups.at[0])
-        out_hid[spot, 1 - side] = hidden_of(gathered, spot, stat, gates.at[1], ups.at[1])
+        factor = factors(stat, spot)
+        out_hid[spot, side] = hidden_of(gathered, spot, factor, gates.at[0], ups.at[0])
+        out_hid[spot, 1 - side] = hidden_of(gathered, spot, factor, gates.at[1], ups.at[1])
         hid_copy(spot).start()
 
     def sh_copy(u):
@@ -704,7 +713,7 @@
         )
 
     def answer(u):
-        out_sh[u] = hidden_of(beside, u, stat_b, s_gate, s_up)
+        out_sh[u] = hidden_of(beside, u, factors(stat_b, u), s_gate, s_up)
         sh_copy(u).start()
 
     def turn(e, carry):
@@ -729,8 +738,9 @@
                 one.wait_recv()
                 onward.start()
             pass_down(1)
-            in_sh[mine] = hidden_of(gathered, place, stat, s_gate, s_up)
-            in_hid[place, side] = hidden_of(gathered, place, stat, gates.at[0], ups.at[0])
+            factor = factors(stat, place)
+            in_sh[mine] = hidden_of(gathered, place, factor, s_gate, s_up)
+            in_hid[place, side] = hidden_of(gathered, place, factor, gates.at[0], ups.at[0])
             for one in pair_weights_on(other_at):
                 one.wait_recv()
 
@@ -748,7 +758,9 @@
         def _():
             down_pair(pair).wait_recv()
             down_core(pair, core).start()
-            in_hid[place, 1 - side] = hidden_of(gathered, place, stat, gates.at[1], ups.at[1])
+            in_hid[place, 1 - side] = hidden_of(
+                gathered, place, factors(stat, place), gates.at[1], ups.at[1]
+            )
             u = across
             for kind in range(2):
                 beside_on(u, kind).wait_recv()
@@ -853,6 +865,7 @@
     early = [s for s in range(segments) if s != last]
     for s in early:
         unit_copy(s).wait_recv()
+    pl.when(place != 0)(lambda: unit_copy(last).wait_recv())
 
     def fin_copy(i):
         return mesh_copy(out_fin.at[i], in_fin.at[i], send_f.at[0], recv_f.at[i], "tp", across)
@@ -863,6 +876,10 @@
             out.at[:, pl.ds(pl.multiple_of(spot * fine, fine), fine)],
             save.at[spot],
         )
+
+    def close(spot, terms):
+        result[spot] = (resid[spot].astype(jnp.float32) + terms).astype(jnp.bfloat16)
+        put(spot).start()
 
     count = half // fine
     mine_at, other_of = far * count, (1 - far) * count
@@ -877,16 +894,23 @@
             for s in early
         ]
         both = sum(terms[1:], terms[0])
-        partial[i] = both
 
         @pl.when(place == 0)
         def _():
+            partial[i] = both[:rows]
             out_fin[i] = both[rows:].astype(jnp.bfloat16)
             fin_copy(i).start()
 
-    def close(spot, terms):
-        result[spot] = (resid[spot].astype(jnp.float32) + terms).astype(jnp.bfloat16)
-        put(spot).start()
+        @pl.when(place != 0)
+        def _():
+            full = both + jnp.dot(
+                units[:, last].reshape(2 * rows, seg),
+                wall[last * seg : (last + 1) * seg, cut],
+                preferred_element_type=jnp.float32,
+            )
+            out_fin[i] = full[rows:].astype(jnp.bfloat16)
+            fin_copy(i).start()
+            close(mine_at + i, full[:rows])
 
     @pl.when(place == 0)
     def _():
@@ -901,23 +925,12 @@
             terms = jnp.dot(
                 rest, wall[last * seg : (last + 1) * seg, cut], preferred_element_type=jnp.float32
             )
-            close(mine_at + i, partial[i, :rows] + terms)
+            close(mine_at + i, partial[i] + terms)
             terms = jnp.dot(rest, extra[:, cut], preferred_element_type=jnp.float32)
             close(other_of + i, in_fin[i].astype(jnp.float32) + terms)
 
     @pl.when(place != 0)
     def _():
-        unit_copy(last).wait_recv()
-        for i in range(count):
-            cut = slice(i * fine, (i + 1) * fine)
-            both = partial[i] + jnp.dot(
-                units[:, last].reshape(2 * rows, seg),
-                wall[last * seg : (last + 1) * seg, cut],
-                preferred_element_type=jnp.float32,
-            )
-            out_fin[i] = both[rows:].astype(jnp.bfloat16)
-            fin_copy(i).start()
-            close(mine_at + i, both[:rows])
         for i in range(count):
             fin_copy(i).wait_recv()
             close(other_of + i, in_fin[i].astype(jnp.float32))
@@ -1025,8 +1038,7 @@
     half, fine = width // 2, width // 8
     seg = 2 * hid
     segments = depth + nt * wide // seg
-    chosen = routes.T[None, :, :] == jnp.arange(n, dtype=jnp.int32)[:, None, None]
-    mix_t = jnp.sum(jnp.where(chosen, route_w.T[None, :, :], 0.0), axis=1)
+    topk = routes.shape[1]
     smem = pl.BlockSpec(memory_space=pltpu.SMEM)
     hbm = pl.BlockSpec(memory_space=pl.ANY)
     low, high = jnp.bfloat16, jnp.float32
@@ -1034,7 +1046,7 @@
     return pl.pallas_call(
         functools.partial(near_kernel, n, nt, group, pieces),
         out_shape=jax.ShapeDtypeStruct((rows, width), low),
-        in_specs=[hbm] * 5 + [smem] + [hbm] * 10,
+        in_specs=[hbm] * 5 + [smem] + [hbm] * 11,
         out_specs=hbm,
         scratch_shapes=[
             pltpu.VMEM((seq, group * HEAD), low),
@@ -1044,7 +1056,8 @@
             pltpu.VMEM((seq, value_dim), low),
             pltpu.VMEM((rows, width), low),
             pltpu.VMEM((1, width), high),
-            pltpu.VMEM((n, rows), high),
+            pltpu.VMEM((topk, rows), jnp.int32),
+            pltpu.VMEM((topk, rows), high),
             pltpu.VMEM((2, tall, HEAD), low),
             pltpu.VMEM((n, seq, HEAD), low),
             pltpu.VMEM((n, seq, HEAD), low),
@@ -1067,8 +1080,8 @@
             pltpu.VMEM((n * hid + nt * wide, half), low),
             pltpu.VMEM((depth, pieces, rows, span), low),
             pltpu.VMEM((nt, pieces, rows, span), low),
-            pltpu.VMEM((depth, rows, HEAD), high),
-            pltpu.VMEM((nt, rows, HEAD), high),
+            pltpu.VMEM((depth, 8, HEAD), high),
+            pltpu.VMEM((nt, 8, HEAD), high),
             pltpu.VMEM((depth, 2, rows, hid), low),
             pltpu.VMEM((depth, 2, rows, hid), low),
             pltpu.VMEM((nt, rows, wide), low),
@@ -1080,8 +1093,8 @@
             pltpu.VMEM((n, rows, HEAD), high),
             pltpu.VMEM((HEAD, HEAD), high),
             pltpu.VMEM((2 * hid, half), low),
-            pltpu.VMEM((half // fine, 2 * rows, fine), high),
-            dma((15,)),
+            pltpu.VMEM((half // fine, rows, fine), high),
+            dma((16,)),
             dma((2, 3, depth)),
             dma((3, n)),
             dma((1,)),
@@ -1116,7 +1129,7 @@
         name="layer",
     )(
         q_first, q_second, k_first, k_second, values, head_lambda, w_out, stream_in,
-        norm_gain.reshape(1, width), mix_t, w_gate[0], w_up[0], s_gate, s_up, w_down[0], s_down,
+        norm_gain.reshape(1, width), routes.T, route_w.T, w_gate[0], w_up[0], s_gate, s_up, w_down[0], s_down,
     )
 
 

time: 93.5 us -> 89.9 us (0.961); the launches traced: 92.2 us -> 89.7 us
  other arithmetic: 1.3 us -> 0 us
  Pallas kernels: 89 us -> 87.8 us
    reduce_sum x1 -> x0, other arithmetic: 1.3 us -> none  [near(): mix_t = jnp.sum(jnp.where(chosen, route_w.T[None, :, :], 0.0), axis=1)]
    pallas_call x1, Pallas kernels: 89 us -> 87.8 us  [near(): pl.pallas_call(functools.partial(near_kernel, n, nt, group, pieces), out_...]
where the time goes in v3:
time: 89.9 us; the launch traced here: 89.7 us
  Pallas kernels  87.8 us (98%)
  local copies, waits for them, and re-layouts  1.87 us (2%)
    pallas_call x1, Pallas kernels, near(): pl.pallas_call(functools.partial(near_kernel, n, nt, group, pieces), out_...  87.8 us
    unnamed x1, local copies, waits for them, and re-layouts  1.87 us

profile of v3, /device:TPU:0, one launch (start us, length us, event | category | flops | bytes accessed | tf_op | source)
XLA Modules:
  0.0 89.7 jit_solution(4608982071393852377)
XLA Ops:
  0.0 87.8 %layer.1 = bf16[64,4096]{1,0:T(8,128)(2,1)} custom-call(bf16[256,256]{1,0:T(8,128)(2,1)} %q_one_h.1, bf16[256,256]{1,0:T(8,128)(2,1)} %q_two_h.1, bf16[256,128]{1,0:T(8,128)(2,1)} %k_one_h.1, bf16[256,128]{1,0:T(8,128)(2,1)} %k_two_h.1, bf16[256,256]{1,0:T(8,128)(2,1)} %val_h.1, f32[2]{0:T(128)} %lam.1, bf16[512,4096]{1,0:T(8,128)(2,1)} %w_out_h.1, ...), custom_call_target="tpu_custom_call" | custom-call | tf_op jit(solution)/shard_map/layer/pallas_call | solution.py:1046
  87.8 1.9 %copy.19 = bf16[64,4096]{1,0:T(8,128)(2,1)} copy(bf16[64,4096]{1,0:T(8,128)(2,1)} %layer.1) | data formatting | bytes 1048576

commit v4 on v3

--- a/solution.py
+++ b/solution.py
@@ -228,8 +228,8 @@
     q_one_h, q_two_h, k_one_h, k_two_h, val_h, lam, w_out_h, stream_h, gain_h, route_h, share_h,
     gate_h, up_h, s_gate_h, s_up_h, down_h, s_down_h,
     out,
-    q_one, q_two, k_one, k_two, val, stream, gain, route_t, share_t,
-    stacked, keys_one, keys_two, vals, peak, total, accum, rows_in,
+    q_one, q_two, k_own, val, stream, gain, route_t, share_t,
+    stacked, keys, vals, peak, total, accum, rows_in,
     w, order, out_one, in_one, out_two, in_two, resid,
     gates, ups, s_gate, s_up, wall, gathered, beside, stat, stat_b,
     out_hid, in_hid, out_sh, in_sh, units, out_fin, in_fin, result, mix, square, extra, partial,
@@ -285,8 +285,8 @@
         pltpu.make_async_copy(source, target, load.at[7 + i])
         for i, (source, target) in enumerate(
             (
-                (k_one_h, k_one),
-                (k_two_h, k_two),
+                (k_one_h, k_own.at[0]),
+                (k_two_h, k_own.at[1]),
                 (val_h, val),
                 (q_one_h, q_one),
                 (q_two_h, q_two),
@@ -303,14 +303,16 @@
         one.wait()
     pl.semaphore_wait(pltpu.get_barrier_semaphore(), depth + 2)
 
-    sources = (k_one, k_two, val)
-    held = (keys_one, keys_two, vals)
+    mid = seq // 2
+
+    def stuff(block):
+        return keys.at[block], vals.at[block, :mid], vals.at[block, mid:]
 
     def copies(block, way, target, own):
         return [
             mesh_copy(
-                sources[a] if own else held[a].at[block],
-                held[a].at[block],
+                (k_own, val.at[:mid], val.at[mid:])[a] if own else stuff(block)[a],
+                stuff(block)[a],
                 send_kv.at[way, a, block // 2],
                 recv_kv.at[a, block],
                 "sp",
@@ -357,7 +359,7 @@
             down_h.at[pl.ds(pl.multiple_of(core * part, part), part), cols_of(far)],
             down_at(me, core),
             send_d.at[way],
-            recv_d.at[0, me],
+            recv_d.at[me],
             "sp",
             target,
         )
@@ -367,7 +369,7 @@
             down_at(block, core),
             down_at(block, core),
             send_d.at[depth + block // 2],
-            recv_d.at[0, block],
+            recv_d.at[block],
             "sp",
             pair,
         )
@@ -376,8 +378,8 @@
         return mesh_copy(
             down_at(block, c),
             down_at(block, c),
-            send_d.at[3 * depth + block],
-            recv_d.at[1, block],
+            send_d.at[3 * depth],
+            recv_d.at[n],
             "tp",
             partner,
         )
@@ -448,10 +450,10 @@
         for h in range(group):
             stacked[index, h * seq : (h + 1) * seq, :] = q[:, h * HEAD : (h + 1) * HEAD]
 
-    def scores_of(index, keys):
+    def scores_of(index, some):
         return (
             lax.dot_general(
-                stacked[index], keys, (((1,), (1,)), ((), ())), preferred_element_type=jnp.float32
+                stacked[index], some, (((1,), (1,)), ((), ())), preferred_element_type=jnp.float32
             )
             * scale
         )
@@ -459,8 +461,8 @@
     spread = (group * seq, seq)
     row_of = lax.broadcasted_iota(jnp.int32, spread, 0) % seq
     allowed = lax.broadcasted_iota(jnp.int32, spread, 1) <= row_of
-    for index, keys in enumerate((k_one, k_two)):
-        scores = jnp.where(allowed, scores_of(index, keys[...]), FLOOR)
+    for index in range(2):
+        scores = jnp.where(allowed, scores_of(index, k_own[index]), FLOOR)
         top = jnp.max(scores, axis=-1, keepdims=True)
         weights = jnp.exp(scores - top)
         peak[index] = top
@@ -471,7 +473,7 @@
 
     def fold(block):
         for index in range(2):
-            scores = scores_of(index, held[index][block])
+            scores = scores_of(index, keys[block, index])
             old = peak[index]
             top = jnp.maximum(old, jnp.max(scores, axis=-1, keepdims=True))
             weights = jnp.exp(scores - top)
@@ -487,7 +489,7 @@
             down_at(block, core),
             down_at(block, core),
             send_d.at[2 * depth + block // 2],
-            recv_d.at[0, block],
+            recv_d.at[block],
             "sp",
             me + 2,
         )
@@ -642,13 +644,13 @@
     square[0:rows, :] = jnp.broadcast_to(shrink, (rows, HEAD))
     stat[place] = square[...].T[0 : stat.shape[1], :]
     rows_out(pieces)
+    ahead = pieces // 2
     for e in range(1, depth - 1):
-        for i in range(pieces + 1):
+        for i in range(pieces + 1 if e == 1 else ahead):
             pl.when(above & (place >= e))(lambda: raise_row(e, i))
-            if e == depth - 2:
+        if e == 1:
+            for i in range(pieces + 1):
                 pl.when(above & below)(lambda: lower_row(1, i))
-
-
     def pass_down(e):
         def one(block, fresh):
             pl.when(fresh)(lambda: down_pair(block).wait_recv())
@@ -685,6 +687,15 @@
         gate_part, up_part = project(g), project(u)
         return (gate_part / (1.0 + jnp.exp(-gate_part)) * up_part).astype(jnp.bfloat16)
 
+    for one, onward in zip(pair_weights(), pair_weights_on(share_at)):
+        one.wait_recv()
+        onward.start()
+    for d in range(1, depth):
+        pass_down(d)
+    for e in range(2, depth - 1):
+        for i in range(pieces + 1):
+            pl.when(below & (place + e < depth))(lambda: lower_row(e, i))
+
     square[...] = jnp.zeros_like(square)
     for j in range(n):
         chosen = jnp.where(route_t[...] == j, share_t[...], 0.0)
@@ -707,6 +718,27 @@
         out_hid[spot, 1 - side] = hidden_of(gathered, spot, factor, gates.at[1], ups.at[1])
         hid_copy(spot).start()
 
+    def serve_last(spot):
+        sums = None
+        mats = (gates.at[0], ups.at[0], gates.at[1], ups.at[1])
+        for i in range(pieces):
+            row_copy(spot, 0, pair, i).wait_recv()
+            parts = [
+                jnp.dot(
+                    gathered[spot, i],
+                    m[i * span : (i + 1) * span, :],
+                    preferred_element_type=jnp.float32,
+                )
+                for m in mats
+            ]
+            sums = parts if sums is None else [a + b for a, b in zip(sums, parts)]
+        row_copy(spot, 0, pair, pieces).wait_recv()
+        factor = factors(stat, spot)
+        g_one, u_one, g_two, u_two = [v * factor for v in sums]
+        for which, g, u in ((side, g_one, u_one), (1 - side, g_two, u_two)):
+            out_hid[spot, which] = (g / (1.0 + jnp.exp(-g)) * u).astype(jnp.bfloat16)
+        hid_copy(spot).start()
+
     def sh_copy(u):
         return mesh_copy(
             out_sh.at[u], in_sh.at[mine], send_s.at[u], recv_s.at[mine], "tp", u
@@ -724,20 +756,13 @@
             for i in range(pieces + 1):
                 row_copy(place - e, 0, pair, i).wait_recv()
 
-        @pl.when(high)
+        @pl.when(high & jnp.logical_not(below))
         def _():
             for i in range(pieces + 1):
-                pl.when(below & (e > 1))(lambda: lower_row(e, i))
-                pl.when(jnp.logical_not(below))(
-                    lambda: row_copy(place + e, 0, pair, i).wait_recv()
-                )
+                row_copy(place + e, 0, pair, i).wait_recv()
 
         @pl.when(e == 1)
         def _():
-            for one, onward in zip(pair_weights(), pair_weights_on(share_at)):
-                one.wait_recv()
-                onward.start()
-            pass_down(1)
             factor = factors(stat, place)
             in_sh[mine] = hidden_of(gathered, place, factor, s_gate, s_up)
             in_hid[place, side] = hidden_of(gathered, place, factor, gates.at[0], ups.at[0])
@@ -752,7 +777,11 @@
         def _():
             serve(place + e)
 
-        pass_down(e + 1)
+        @pl.when(e == 1)
+        def _():
+            for d in range(2, depth - 1):
+                for i in range(ahead, pieces + 1):
+                    pl.when(above & (place >= d))(lambda: raise_row(d, i))
 
         @pl.when(e == 2)
         def _():
@@ -787,9 +816,7 @@
 
     @pl.when(place == 0)
     def _():
-        for i in range(pieces + 1):
-            row_copy(last, 0, pair, i).wait_recv()
-        serve(last)
+        serve_last(last)
 
     segments = units.shape[1]
 
@@ -838,9 +865,7 @@
 
     @pl.when(top_place)
     def _():
-        for i in range(pieces + 1):
-            row_copy(0, 0, pair, i).wait_recv()
-        serve(0)
+        serve_last(0)
 
     @pl.when(place == 0)
     def _():
@@ -854,14 +879,9 @@
     for o in range(2):
         sd_on(2 * ((far + o) % 2) + 1 - core).wait_recv()
 
-    def receive_down(block, carry):
-        @pl.when(block != me)
-        def _():
-            down_core(block, 1 - core).wait_recv()
-
-        return carry
-
-    lax.fori_loop(0, n, receive_down, 0)
+    taken = wall.at[pl.ds(0, (n - 1) * part)]
+    cores = mesh_copy(taken, taken, send_d.at[3 * depth], recv_d.at[n], "tp", partner)
+    cores.wait_recv()
     early = [s for s in range(segments) if s != last]
     for s in early:
         unit_copy(s).wait_recv()
@@ -874,7 +894,7 @@
         return pltpu.make_async_copy(
             result.at[spot],
             out.at[:, pl.ds(pl.multiple_of(spot * fine, fine), fine)],
-            save.at[spot],
+            save.at[0],
         )
 
     def close(spot, terms):
@@ -966,14 +986,7 @@
 
     lax.fori_loop(0, depth, settle, 0)
 
-    def settle_down(block, carry):
-        @pl.when(block != me)
-        def _():
-            down_core(block, core).wait_send()
-
-        return carry
-
-    lax.fori_loop(0, n, settle_down, 0)
+    cores.wait_send()
     for one in pair_weights() + pair_weights_on(share_at):
         one.wait_send()
     for some, sem, rec in (
@@ -1004,8 +1017,7 @@
         extra_core(0, core).wait_send()
         extra_core(1, core).wait_send()
 
-    for i in range(2 * count):
-        put(i).wait()
+    pltpu.make_async_copy(stream_h, stream, save.at[0]).wait()
 
 
 def near(
@@ -1051,16 +1063,14 @@
         scratch_shapes=[
             pltpu.VMEM((seq, group * HEAD), low),
             pltpu.VMEM((seq, group * HEAD), low),
-            pltpu.VMEM((seq, HEAD), low),
-            pltpu.VMEM((seq, HEAD), low),
+            pltpu.VMEM((2, seq, HEAD), low),
             pltpu.VMEM((seq, value_dim), low),
             pltpu.VMEM((rows, width), low),
             pltpu.VMEM((1, width), high),
             pltpu.VMEM((topk, rows), jnp.int32),
             pltpu.VMEM((topk, rows), high),
             pltpu.VMEM((2, tall, HEAD), low),
-            pltpu.VMEM((n, seq, HEAD), low),
-            pltpu.VMEM((n, seq, HEAD), low),
+            pltpu.VMEM((n, 2, seq, HEAD), low),
             pltpu.VMEM((n, seq, value_dim), low),
             pltpu.VMEM((2, tall, 1), high),
             pltpu.VMEM((2, tall, 1), high),
@@ -1103,8 +1113,8 @@
             dma((pieces,)),
             dma((2, 2)),
             dma((2, 2)),
-            dma((3 * depth + n,)),
-            dma((2, n)),
+            dma((3 * depth + 1,)),
+            dma((n + 1,)),
             dma((3,)),
             dma((nt,)),
             dma((2, 2, depth)),
@@ -1119,7 +1129,7 @@
             dma((segments,)),
             dma((1,)),
             dma((half // fine,)),
-            dma((width // fine,)),
+            dma((1,)),
             dma((4,)),
             dma((2, 2)),
         ],

time: 89.9 us -> 87.6 us (0.974); the launches traced: 89.7 us -> 86.4 us
  Pallas kernels: 87.8 us -> 84.6 us
    pallas_call x1, Pallas kernels: 87.8 us -> 84.6 us  [near(): pl.pallas_call(functools.partial(near_kernel, n, nt, group, pieces), out_...]
where the time goes in v4:
time: 87.6 us; the launch traced here: 86.4 us
  Pallas kernels  84.6 us (97%)
  local copies, waits for them, and re-layouts  1.87 us (2%)
    pallas_call x1, Pallas kernels, near(): pl.pallas_call(functools.partial(near_kernel, n, nt, group, pieces), out_...  84.6 us
    unnamed x1, local copies, waits for them, and re-layouts  1.87 us

profile of v4, /device:TPU:0, one launch (start us, length us, event | category | flops | bytes accessed | tf_op | source)
XLA Modules:
  0.0 86.4 jit_solution(16395728067074274681)
XLA Ops:
  0.0 84.6 %layer.1 = bf16[64,4096]{1,0:T(8,128)(2,1)} custom-call(bf16[256,256]{1,0:T(8,128)(2,1)} %q_one_h.1, bf16[256,256]{1,0:T(8,128)(2,1)} %q_two_h.1, bf16[256,128]{1,0:T(8,128)(2,1)} %k_one_h.1, bf16[256,128]{1,0:T(8,128)(2,1)} %k_two_h.1, bf16[256,256]{1,0:T(8,128)(2,1)} %val_h.1, f32[2]{0:T(128)} %lam.1, bf16[512,4096]{1,0:T(8,128)(2,1)} %w_out_h.1, ...), custom_call_target="tpu_custom_call" | custom-call | tf_op jit(solution)/shard_map/layer/pallas_call | solution.py:1058
  84.6 1.9 %copy.19 = bf16[64,4096]{1,0:T(8,128)(2,1)} copy(bf16[64,4096]{1,0:T(8,128)(2,1)} %layer.1) | data formatting | bytes 1048576

commit v5 on v4

--- a/solution.py
+++ b/solution.py
@@ -693,7 +693,7 @@
     for d in range(1, depth):
         pass_down(d)
     for e in range(2, depth - 1):
-        for i in range(pieces + 1):
+        for i in range(ahead):
             pl.when(below & (place + e < depth))(lambda: lower_row(e, i))
 
     square[...] = jnp.zeros_like(square)
@@ -782,6 +782,7 @@
             for d in range(2, depth - 1):
                 for i in range(ahead, pieces + 1):
                     pl.when(above & (place >= d))(lambda: raise_row(d, i))
+                    pl.when(below & (place + d < depth))(lambda: lower_row(d, i))
 
         @pl.when(e == 2)
         def _():
@@ -825,20 +826,21 @@
             units.at[0, s], units.at[1, s], send_u.at[s], recv_u.at[s], "tp", across
         )
 
-    for o in range(1, nt):
-        u = (mine + o) % nt
-        mesh_copy(
-            out_sh.at[u], in_sh.at[u], send_s.at[u], recv_s.at[u], "tp", u
-        ).wait_recv()
     seg = units.shape[3]
-    for j in range(nt):
-        at = j * wide
-        units[0, depth + at // seg, :, at % seg : at % seg + wide] = in_sh[j]
-    for s in range(depth, segments):
-        unit_copy(s).start()
-
-    for e in range(1, depth - 1):
-        collect(e)
+
+    def share_units():
+        for o in range(1, nt):
+            u = (mine + o) % nt
+            mesh_copy(
+                out_sh.at[u], in_sh.at[u], send_s.at[u], recv_s.at[u], "tp", u
+            ).wait_recv()
+        for j in range(nt):
+            at = j * wide
+            units[0, depth + at // seg, :, at % seg : at % seg + wide] = in_sh[j]
+        for s in range(depth, segments):
+            unit_copy(s).start()
+
+    pl.when(top_place)(share_units)
 
     def place_unit(spot):
         @pl.when(place != spot)
@@ -854,15 +856,21 @@
                 in_hid[spot, k].astype(jnp.float32) * mix[j][:, :1]
             ).astype(jnp.bfloat16)
 
-    for spot in range(last - 1, -1, -1):
-        place_unit(spot)
-        unit_copy(spot).start()
-
     @pl.when(place != 0)
     def _():
         place_unit(last)
         unit_copy(last).start()
 
+    for spot in range(last - 1, -1, -1):
+        place_unit(spot)
+        unit_copy(spot).start()
+
+    pl.when(jnp.logical_not(top_place))(share_units)
+    for e in range(1, depth - 1):
+        collect(e)
+
+    collect(last)
+
     @pl.when(top_place)
     def _():
         serve_last(0)
@@ -872,7 +880,6 @@
         extra_pair(1 - side).wait_recv()
         extra_core(1 - side, core).start()
 
-    collect(last)
 
     loads[5].wait()
     loads[6].wait()

time: 87.6 us -> 86.6 us (0.989); the launches traced: 86.4 us -> 86.4 us
  no operation moved by 1% of the time
where the time goes in v5:
time: 86.6 us; the launch traced here: 86.4 us
  Pallas kernels  84.6 us (98%)
  local copies, waits for them, and re-layouts  1.87 us (2%)
    pallas_call x1, Pallas kernels, near(): pl.pallas_call(functools.partial(near_kernel, n, nt, group, pieces), out_...  84.6 us
    unnamed x1, local copies, waits for them, and re-layouts  1.87 us

profile of v5, /device:TPU:0, one launch (start us, length us, event | category | flops | bytes accessed | tf_op | source)
XLA Modules:
  0.0 86.4 jit_solution(8394321001198606304)
XLA Ops:
  0.0 84.6 %layer.1 = bf16[64,4096]{1,0:T(8,128)(2,1)} custom-call(bf16[256,256]{1,0:T(8,128)(2,1)} %q_one_h.1, bf16[256,256]{1,0:T(8,128)(2,1)} %q_two_h.1, bf16[256,128]{1,0:T(8,128)(2,1)} %k_one_h.1, bf16[256,128]{1,0:T(8,128)(2,1)} %k_two_h.1, bf16[256,256]{1,0:T(8,128)(2,1)} %val_h.1, f32[2]{0:T(128)} %lam.1, bf16[512,4096]{1,0:T(8,128)(2,1)} %w_out_h.1, ...), custom_call_target="tpu_custom_call" | custom-call | tf_op jit(solution)/shard_map/layer/pallas_call | solution.py:1065
  84.6 1.9 %copy.19 = bf16[64,4096]{1,0:T(8,128)(2,1)} copy(bf16[64,4096]{1,0:T(8,128)(2,1)} %layer.1) | data formatting | bytes 1048576

commit v6 on v5

--- a/solution.py
+++ b/solution.py
@@ -644,7 +644,7 @@
     square[0:rows, :] = jnp.broadcast_to(shrink, (rows, HEAD))
     stat[place] = square[...].T[0 : stat.shape[1], :]
     rows_out(pieces)
-    ahead = pieces // 2
+    ahead = pieces // 4
     for e in range(1, depth - 1):
         for i in range(pieces + 1 if e == 1 else ahead):
             pl.when(above & (place >= e))(lambda: raise_row(e, i))
@@ -1052,7 +1052,7 @@
     group, value_dim = q_first.shape[1] // HEAD, values.shape[1]
     hid, wide = w_down.shape[1], s_down.shape[0]
     tall, features = group * seq, group * value_dim
-    pieces = 4
+    pieces = 8
     span = width // pieces
     half, fine = width // 2, width // 8
     seg = 2 * hid

time: 86.6 us -> 86.4 us (level); the launches traced: 86.4 us -> 85.3 us
  Pallas kernels: 84.6 us -> 83.5 us
    pallas_call x1, Pallas kernels: 84.6 us -> 83.5 us  [near(): pl.pallas_call(functools.partial(near_kernel, n, nt, group, pieces), out_...]
where the time goes in v6:
time: 86.4 us; the launch traced here: 85.3 us
  Pallas kernels  83.5 us (97%)
  local copies, waits for them, and re-layouts  1.87 us (2%)
    pallas_call x1, Pallas kernels, near(): pl.pallas_call(functools.partial(near_kernel, n, nt, group, pieces), out_...  83.5 us
    unnamed x1, local copies, waits for them, and re-layouts  1.87 us

profile of v6, /device:TPU:0, one launch (start us, length us, event | category | flops | bytes accessed | tf_op | source)
XLA Modules:
  0.0 85.3 jit_solution(10754113486648516732)
XLA Ops:
  0.0 83.5 %layer.1 = bf16[64,4096]{1,0:T(8,128)(2,1)} custom-call(bf16[256,256]{1,0:T(8,128)(2,1)} %q_one_h.1, bf16[256,256]{1,0:T(8,128)(2,1)} %q_two_h.1, bf16[256,128]{1,0:T(8,128)(2,1)} %k_one_h.1, bf16[256,128]{1,0:T(8,128)(2,1)} %k_two_h.1, bf16[256,256]{1,0:T(8,128)(2,1)} %val_h.1, f32[2]{0:T(128)} %lam.1, bf16[512,4096]{1,0:T(8,128)(2,1)} %w_out_h.1, ...), custom_call_target="tpu_custom_call" | custom-call | tf_op jit(solution)/shard_map/layer/pallas_call | solution.py:1065
  83.5 1.9 %copy.19 = bf16[64,4096]{1,0:T(8,128)(2,1)} copy(bf16[64,4096]{1,0:T(8,128)(2,1)} %layer.1) | data formatting | bytes 1048576
